TPU v7x, 32 devices: a whole 2x2x4 slice. The times are simulated.
32 devices in a mesh: sp: 16 (over z, y, core), tp: 2 (over x).
Axes of the slice: x: 2, y: 2, z: 4, core: 2. Of those that a mesh axis runs over, the one named last changes fastest.
Arguments:
- residual: bfloat16 [2048, 2048], P('sp', 'tp'), may hold values from -24 to 24
- queries: bfloat16 [2048, 2048], P('sp', 'tp'), may hold values from -16 to 16
- key_proj: bfloat16 [2048, 512], P(('sp', 'tp')), may hold values from -8 to 8
- value_proj: bfloat16 [2048, 512], P(('sp', 'tp')), may hold values from -6 to 6
- diff_lambda: float32 [8], replicated, may hold values from 0.3 to 0.8
- head_gain: float32 [256], replicated, may hold values from 0.1 to 1.9
- out_weight: bfloat16 [2048, 2048], P(None, 'tp'), may hold values from -0.125 to 0.125
- norm_gain: float32 [2048], P('tp'), may hold values from 0.1 to 1.9
- up_weight: bfloat16 [2048, 8192], P('sp', 'tp'), may hold values from -0.125 to 0.125
- down_weight: bfloat16 [8192, 2048], P('tp', 'sp'), may hold values from -0.0625 to 0.0625
Outputs:
- layer_out: bfloat16 [2048, 2048], P('sp', 'tp')
All inputs are finite; a program needn't handle non-finite values.
Results may differ from a plain program's by a relative error of at most 0.012.
Values may be sent and summed in bfloat16 or wider, within the bound.
A program may use at most 128 MiB of HBM per device.

v0:
```python
import functools
import math

import jax
import jax.numpy as jnp
from jax import lax
from jax.experimental import pallas as pl
from jax.experimental.pallas import tpu as pltpu
from jax.sharding import PartitionSpec as P

D = 2048
HEADS = 8
KV_HEADS = 2
HEAD_DIM = 128
VALUE_DIM = 256


epsilon = 1e-06


def head_norm(per_map, lambdas, gain):
    difference = per_map[:, 0] - lambdas[:, None, None] * per_map[:, 1]
    scaled = (
        difference
        * lax.rsqrt(jnp.mean(difference * difference, axis=-1, keepdims=True) + epsilon)
        * gain
    )
    return scaled.astype(jnp.bfloat16)


def on_device(
    residual,
    queries,
    key_proj,
    value_proj,
    diff_lambda,
    head_gain,
    out_weight,
    norm_gain,
    up_weight,
    down_weight,
):
    rows_here = residual.shape[0]
    per_group = HEADS // KV_HEADS
    scaling = HEAD_DIM ** (-0.5)
    all_queries = lax.all_gather(queries, "tp", axis=1, tiled=True)
    query_grid = all_queries.reshape(rows_here, KV_HEADS, per_group, 2, HEAD_DIM)
    stat_shape = (KV_HEADS, per_group, 2, rows_here)
    maxima = jnp.full(stat_shape, -1e30, jnp.float32)
    key_piece = lax.all_gather(key_proj, "sp", axis=0, tiled=True)
    value_piece = lax.all_gather(value_proj, "sp", axis=0, tiled=True)
    key_count = key_piece.shape[0]
    key_grid = key_piece.reshape(key_count, KV_HEADS, 2, HEAD_DIM)
    value_grid = value_piece.reshape(key_count, KV_HEADS, VALUE_DIM)
    scores = (
        jnp.einsum("qagcd,kacd->agcqk", query_grid, key_grid, preferred_element_type=jnp.float32)
        * scaling
    )
    highest = jnp.maximum(maxima, jnp.max(scores, axis=-1))
    weights = jnp.exp(scores - highest[..., None])
    totals = jnp.sum(weights, axis=-1)
    weighted = jnp.einsum(
        "agcqk,kae->agcqe",
        weights.astype(jnp.bfloat16),
        value_grid,
        preferred_element_type=jnp.float32,
    )
    maxima, totals, weighted = (highest, totals, weighted)
    maxima = maxima.reshape(HEADS, 2, rows_here)
    totals = totals.reshape(HEADS, 2, rows_here)
    weighted = weighted.reshape(HEADS, 2, rows_here, VALUE_DIM)
    tp_size = lax.axis_size("tp")
    local_heads = HEADS // tp_size
    got_max, got_tot, got_sum = (
        lax.all_to_all(maxima, "tp", split_axis=0, concat_axis=0, tiled=True),
        lax.all_to_all(totals, "tp", split_axis=0, concat_axis=0, tiled=True),
        lax.all_to_all(weighted, "tp", split_axis=0, concat_axis=0, tiled=True),
    )
    got_max = got_max.reshape(tp_size, local_heads, 2, rows_here)
    got_tot = got_tot.reshape(tp_size, local_heads, 2, rows_here)
    got_sum = got_sum.reshape(tp_size, local_heads, 2, rows_here, VALUE_DIM)
    highest = jnp.max(got_max, axis=0)
    factor = jnp.exp(got_max - highest)
    totals_all = jnp.sum(factor * got_tot, axis=0)
    sums_all = jnp.sum(factor[..., None] * got_sum, axis=0)
    lambdas = lax.dynamic_slice_in_dim(diff_lambda, lax.axis_index("tp") * local_heads, local_heads)
    own_heads = head_norm(sums_all / totals_all[..., None], lambdas, head_gain)
    head_outputs = lax.all_gather(own_heads, "tp", axis=0, tiled=True)
    out_grid = out_weight.reshape(HEADS, VALUE_DIM, out_weight.shape[1])
    projected = jnp.einsum(
        "hqe,hed->qd", head_outputs, out_grid, preferred_element_type=jnp.float32
    )
    after_mix = residual.astype(jnp.float32) + projected
    squares = lax.psum(jnp.sum(after_mix * after_mix, axis=1), "tp")
    normed = (after_mix * lax.rsqrt(squares / D + epsilon)[:, None] * norm_gain).astype(
        jnp.bfloat16
    )
    full_rows = lax.all_gather(normed, "tp", axis=1, tiled=True)
    hidden = jnp.dot(
        full_rows,
        lax.all_gather(up_weight, "sp", axis=0, tiled=True),
        preferred_element_type=jnp.float32,
    )
    activated = jnp.square(jax.nn.relu(hidden)).astype(jnp.bfloat16)
    partial_value = jnp.dot(
        activated,
        lax.all_gather(down_weight, "sp", axis=1, tiled=True),
        preferred_element_type=jnp.float32,
    )
    mixer_sum = lax.psum_scatter(partial_value, "tp", scatter_dimension=1, tiled=True)
    return (after_mix + mixer_sum).astype(jnp.bfloat16)


MESH = pl.DeviceIdType.MESH
F32 = jnp.float32
BF16 = jnp.bfloat16
CHIP_CORES = 2
Y_CHIPS = 2


def fused_kernel(
    layers, residual, queries, keys, values, lambdas, head_gain, out_weight, norm_gain,
    up, down, out,
    kv_all, up_all, down_all, q_buf, res_buf, w_buf, heads_all, squares, tokens,
    part_out, part_in, sum_out, sum_in, after, own_part, local_sem, send_sem, recv_sem,
):
    x = lax.axis_index("tp")
    s = lax.axis_index("sp")
    core, y, z = s % CHIP_CORES, (s // CHIP_CORES) % Y_CHIPS, s // (CHIP_CORES * Y_CHIPS)

    def place(z_, y_, c_):
        return (z_ * Y_CHIPS + y_) * CHIP_CORES + c_

    def z_back(d):
        return lax.rem(z - d + layers, layers)

    def z_ahead(d):
        return lax.rem(z + d, layers)

    mate = {"sp": s, "tp": 1 - x}
    beside = {"sp": place(z, 1 - y, core), "tp": x}
    twin = {"sp": place(z, y, 1 - core), "tp": x}
    column = [{"sp": place(z_ahead(d), y, core), "tp": x} for d in range(layers)]

    barrier = pltpu.get_barrier_semaphore()
    peers = [mate, beside, twin] + column[1:]
    for peer in peers:
        pl.semaphore_signal(barrier, inc=1, device_id=peer, device_id_type=MESH)

    count = {"local": 0, "remote": 0}
    started = []

    def bring(src, dst):
        copy = pltpu.make_async_copy(src, dst, local_sem.at[count["local"]])
        count["local"] += 1
        copy.start()
        return copy

    def send(src, dst, peer):
        i = count["remote"]
        count["remote"] += 1
        copy = pltpu.make_async_remote_copy(
            src_ref=src, dst_ref=dst, send_sem=send_sem.at[i], recv_sem=recv_sem.at[i],
            device_id=peer, device_id_type=MESH,
        )
        copy.start()
        started.append(copy)
        return copy

    few = keys.shape[0]
    kw = kv_all.shape[2] // 2
    chunk = up_all.shape[2]
    lanes = down.shape[1]

    def half(ref, part):
        return ref.at[:, pl.ds(pl.multiple_of(part * kw, kw), kw)]

    def kv_rows(block, part, side):
        return kv_all.at[block, pl.ds(pl.multiple_of(part * few, few), few), pl.ds(side * kw, kw)]

    own_kv = [bring(half(keys, x), kv_rows(s, x, 0)), bring(half(values, x), kv_rows(s, x, 1))]
    q_copy = bring(queries, q_buf)

    pl.semaphore_wait(barrier, len(peers))

    swapped = [
        send(half(keys, 1 - x), kv_rows(s, x, 0), mate),
        send(half(values, 1 - x), kv_rows(s, x, 1), mate),
    ]
    for copy in own_kv:
        copy.wait()
    for copy in swapped:
        copy.wait_recv()
    kv_z = [None] + [send(kv_all.at[s], kv_all.at[s], column[d]) for d in range(1, layers)]

    def up_chunk(part):
        return up.at[:, pl.ds(pl.multiple_of(part * chunk, chunk), chunk)]

    def down_chunk(part):
        return down.at[pl.ds(pl.multiple_of(part * chunk, chunk), chunk), :]

    def up_block(b):
        return up_all.at[b]

    def down_block(b):
        return down_all.at[:, pl.ds(pl.multiple_of(b * lanes, lanes), lanes)]

    up_z = [None] + [send(up_chunk(z_ahead(d)), up_block(s), column[d]) for d in range(1, layers)]
    up_own = bring(up_chunk(z), up_block(s))
    down_own = bring(down_chunk(z), down_block(s))
    w_copy = bring(out_weight, w_buf)
    r_copy = bring(residual, res_buf)

    def spread(block_of, d, arrival):
        if arrival is not None:
            arrival()
        b = block_of(place(z_back(d), y, core))
        return send(b, b, beside), send(b, b, twin)

    def pass_on(block_of, d, came):
        came.wait_recv()
        b = block_of(place(z_back(d), 1 - y, core))
        return send(b, b, twin)

    def kv_block(b):
        return kv_all.at[b]

    up_y, up_t, up_u = {}, {}, {}
    down_y, down_t, down_u = {}, {}, {}
    kv_y, kv_t, kv_u = [], [], []
    for d in range(layers):
        to_y, to_t = spread(kv_block, d, kv_z[d].wait_recv if d else None)
        kv_y.append(to_y)
        kv_t.append(to_t)
        if d:
            kv_u.append(pass_on(kv_block, d - 1, kv_y[d - 1]))
        else:
            up_y[0], up_t[0] = spread(up_block, 0, up_own.wait)
            down_z = [None] + [
                send(down_chunk(z_ahead(e)), down_block(s), column[e]) for e in range(1, layers)
            ]
    kv_u.append(pass_on(kv_block, layers - 1, kv_y[layers - 1]))

    down_y[0], down_t[0] = spread(down_block, 0, down_own.wait)
    for copy in kv_t + kv_u:
        copy.wait_recv()
    q_copy.wait()

    local_heads = q_buf.shape[1] // (2 * HEAD_DIM)
    blocks, per_block = kv_all.shape[0], kv_all.shape[1]
    key_count = blocks * per_block
    factor = HEAD_DIM ** (-0.5) * math.log2(math.e)
    vals = lambda: kv_all[:, :, kw:].reshape(key_count, kw)
    head_copies = []
    for h in range(local_heads):
        maps = []
        for c in range(2):
            q = q_buf[:, (2 * h + c) * HEAD_DIM : (2 * h + c + 1) * HEAD_DIM]
            k = kv_all[:, :, c * HEAD_DIM : (c + 1) * HEAD_DIM].reshape(key_count, HEAD_DIM)
            scores = lax.dot_general(q, k, (((1,), (1,)), ((), ())), preferred_element_type=F32)
            top = jnp.max(scores, axis=1, keepdims=True)
            weights = jnp.exp2((scores - top) * factor)
            total = jnp.sum(weights, axis=1, keepdims=True)
            summed = jnp.dot(weights.astype(BF16), vals(), preferred_element_type=F32)
            maps.append(summed / total)
        diff = maps[0] - lambdas[x * local_heads + h] * maps[1]
        scaled = diff * lax.rsqrt(jnp.mean(diff * diff, axis=1, keepdims=True) + epsilon)
        where = heads_all.at[x, :, pl.ds(h * VALUE_DIM, VALUE_DIM)]
        heads_all[x, :, pl.ds(h * VALUE_DIM, VALUE_DIM)] = (scaled * head_gain[...]).astype(BF16)
        head_copies.append(send(where, where, mate))
        if 1 <= h < layers:
            up_y[h], up_t[h] = spread(up_block, h, up_z[h].wait_recv)
    for d in range(max(local_heads, 1), layers):
        up_y[d], up_t[d] = spread(up_block, d, up_z[d].wait_recv)

    wide = heads_all.shape[2]
    w_copy.wait()
    r_copy.wait()

    def w_rows(part):
        return w_buf[pl.ds(pl.multiple_of(part * wide, wide), wide), :]

    mix = res_buf[...].astype(F32) + jnp.dot(heads_all[x], w_rows(x), preferred_element_type=F32)
    for copy in head_copies:
        copy.wait_recv()
    mix = mix + jnp.dot(heads_all[1 - x], w_rows(1 - x), preferred_element_type=F32)
    after[...] = mix
    own_squares = jnp.sum(mix * mix, axis=1, keepdims=True)
    squares[x] = jnp.broadcast_to(own_squares, squares.shape[1:])
    sq_copy = send(squares.at[x], squares.at[x], mate)
    sq_copy.wait_recv()
    width = 2 * wide
    mean = (own_squares + squares[1 - x][:, :1]) / width
    tokens[z, x] = (after[...] * lax.rsqrt(mean + epsilon) * norm_gain[...]).astype(BF16)

    mine = tokens.at[z, x]
    tok_z = [None] + [send(mine, mine, column[d]) for d in range(1, layers)]
    tok_x = {0: send(mine, mine, mate)}
    for d in range(1, layers):
        up_u[d - 1] = pass_on(up_block, d - 1, up_y[d - 1])
        down_y[d], down_t[d] = spread(down_block, d, down_z[d].wait_recv)
    up_u[layers - 1] = pass_on(up_block, layers - 1, up_y[layers - 1])
    down_u[0] = pass_on(down_block, 0, down_y[0])

    def cross(d):
        tok_z[d].wait_recv()
        block = tokens.at[z_back(d), x]
        tok_x[d] = send(block, block, mate)

    order = list(range(1, layers)) + [0]
    for d in order[:1]:
        cross(d)
    for d in range(1, layers):
        down_u[d] = pass_on(down_block, d, down_y[d])
    for d in order[1:-1][:1]:
        cross(d)
    for group in (up_t, up_u, down_t, down_u):
        for d in range(layers):
            group[d].wait_recv()

    up_half = up_all.shape[0] // 2
    part_copies, sum_copies = {}, {}

    def up_rows(i):
        return up_all[i * up_half : (i + 1) * up_half].reshape(wide, chunk)

    def settle(d):
        part_copies[d].wait_recv()
        both = own_part[d] + part_in[d].astype(F32)
        if d == 0:
            after[...] = after[...] + both
        else:
            sum_out[d - 1] = both.astype(BF16)
            back = {"sp": place(z_back(d), y, core), "tp": x}
            sum_copies[d] = send(sum_out.at[d - 1], sum_in.at[d - 1], back)

    for i, d in enumerate(order):
        zb = z_back(d)
        tok_x[d].wait_recv()
        hidden = jnp.dot(tokens[zb, 0], up_rows(0), preferred_element_type=F32) + jnp.dot(
            tokens[zb, 1], up_rows(1), preferred_element_type=F32
        )
        activated = jnp.square(jnp.maximum(hidden, 0.0)).astype(BF16)

        def down_cols(part):
            return down_all[:, pl.ds(pl.multiple_of(part * wide, wide), wide)]

        part_out[d] = jnp.dot(activated, down_cols(1 - x), preferred_element_type=F32).astype(BF16)
        part_copies[d] = send(part_out.at[d], part_in.at[d], mate)
        own_part[d] = jnp.dot(activated, down_cols(x), preferred_element_type=F32)
        if i + 2 < layers - 1:
            cross(order[i + 2])
        if i:
            settle(order[i - 1])
    settle(order[-1])
    result = after[...]
    for d in range(1, layers):
        sum_copies[d].wait_recv()
        result = result + sum_in[d - 1].astype(F32)
    out[...] = result.astype(out.dtype)
    for copy in started:
        copy.wait_send()


def on_chip(sp_size, residual, queries, key_proj, value_proj, diff_lambda, head_gain, out_weight,
            norm_gain, up_weight, down_weight):
    layers = sp_size // (CHIP_CORES * Y_CHIPS)
    rows, wide = residual.shape
    kw = key_proj.shape[1] // KV_HEADS
    chunk = up_weight.shape[1] // layers
    hbm = pl.BlockSpec(memory_space=pltpu.HBM)
    vmem = pl.BlockSpec(memory_space=pltpu.VMEM)
    smem = pl.BlockSpec(memory_space=pltpu.SMEM)
    copies = 2 + 3 * (layers - 1) + 3 * 3 * layers + wide // VALUE_DIM + 1 + 3 * layers + layers
    return pl.pallas_call(
        functools.partial(fused_kernel, layers),
        out_shape=jax.ShapeDtypeStruct(residual.shape, BF16),
        in_specs=[hbm, hbm, hbm, hbm, smem, vmem, hbm, vmem, hbm, hbm],
        out_specs=vmem,
        scratch_shapes=[
            pltpu.VMEM((sp_size, 2 * key_proj.shape[0], 2 * kw), BF16),
            pltpu.VMEM((sp_size, up_weight.shape[0], chunk), BF16),
            pltpu.VMEM((chunk, sp_size * down_weight.shape[1]), BF16),
            pltpu.VMEM(queries.shape, BF16),
            pltpu.VMEM(residual.shape, BF16),
            pltpu.VMEM(out_weight.shape, BF16),
            pltpu.VMEM((2, rows, wide), BF16),
            pltpu.VMEM((2, rows, 128), F32),
            pltpu.VMEM((layers, 2, rows, wide), BF16),
            pltpu.VMEM((layers, rows, wide), BF16),
            pltpu.VMEM((layers, rows, wide), BF16),
            pltpu.VMEM((layers - 1, rows, wide), BF16),
            pltpu.VMEM((layers - 1, rows, wide), BF16),
            pltpu.VMEM((rows, wide), F32),
            pltpu.VMEM((layers, rows, wide), F32),
            pltpu.SemaphoreType.DMA((8,)),
            pltpu.SemaphoreType.DMA((copies,)),
            pltpu.SemaphoreType.DMA((copies,)),
        ],
        compiler_params=pltpu.CompilerParams(
            collective_id=0, has_side_effects=True, vmem_limit_bytes=60 * 2**20
        ),
        name="fused_layer",
    )(residual, queries, key_proj, value_proj, diff_lambda, head_gain.reshape(1, -1), out_weight,
      norm_gain.reshape(1, -1), up_weight, down_weight)


def solution(mesh):
    sp_size, tp_size = mesh.shape["sp"], mesh.shape["tp"]
    direct = tp_size == KV_HEADS == 2 and sp_size % (CHIP_CORES * Y_CHIPS) == 0
    body = functools.partial(on_chip, sp_size) if direct else on_device
    return jax.shard_map(
        body,
        mesh=mesh,
        in_specs=(
            P("sp", "tp"),
            P("sp", "tp"),
            P(("sp", "tp"), None),
            P(("sp", "tp"), None),
            P(),
            P(),
            P(None, "tp"),
            P("tp"),
            P("sp", "tp"),
            P("tp", "sp"),
        ),
        out_specs=P("sp", "tp"),
        check_vma=False,
    )
```

profile of v0, /device:TPU:0, one launch (start us, length us, event | category | flops | bytes accessed | tf_op | source)
XLA Modules:
  0.0 131.5 jit_solution(11076652639723622613)
XLA Ops:
  0.0 129.8 %fused_layer.1 = bf16[128,1024]{1,0:T(8,128)(2,1)} custom-call(bf16[128,1024]{1,0:T(8,128)(2,1)} %residual.1, bf16[128,1024]{1,0:T(8,128)(2,1)} %queries.1, bf16[64,512]{1,0:T(8,128)(2,1)} %keys.1, bf16[64,512]{1,0:T(8,128)(2,1)} %values.1, f32[8]{0:T(128)} %lambdas.1, f32[1,256]{1,0:T(1,128)} %bitcast.3, bf16[2048,1024]{1,0:T(8,128)(2,1)} %out_weight.1, ...), custom_call_target="tpu_custom_call" | custom-call | tf_op jit(solution)/shard_map/fused_layer/pallas_call | solution.py:375
  129.8 1.7 %copy.12 = bf16[128,1024]{1,0:T(8,128)(2,1)} copy(bf16[128,1024]{1,0:T(8,128)(2,1)} %fused_layer.1) | data formatting | bytes 524288
where the time goes:
time: 132 us; the launch traced here: 131 us
  Pallas kernels  130 us (98%)
  local copies, waits for them, and re-layouts  1.67 us (1%)
    pallas_call x1, Pallas kernels, on_chip(): pl.pallas_call(functools.partial(fused_kernel, layers), out_shape=jax.Sha...  130 us

commit v1 on v0

v1 whole, which is shorter than its diff:
```python
import functools
import math

import jax
import jax.numpy as jnp
from jax import lax
from jax.experimental import pallas as pl
from jax.experimental.pallas import tpu as pltpu
from jax.sharding import PartitionSpec as P

D = 2048
HEADS = 8
KV_HEADS = 2
HEAD_DIM = 128
VALUE_DIM = 256


epsilon = 1e-06


def head_norm(per_map, lambdas, gain):
    difference = per_map[:, 0] - lambdas[:, None, None] * per_map[:, 1]
    scaled = (
        difference
        * lax.rsqrt(jnp.mean(difference * difference, axis=-1, keepdims=True) + epsilon)
        * gain
    )
    return scaled.astype(jnp.bfloat16)


def on_device(
    residual,
    queries,
    key_proj,
    value_proj,
    diff_lambda,
    head_gain,
    out_weight,
    norm_gain,
    up_weight,
    down_weight,
):
    rows_here = residual.shape[0]
    per_group = HEADS // KV_HEADS
    scaling = HEAD_DIM ** (-0.5)
    all_queries = lax.all_gather(queries, "tp", axis=1, tiled=True)
    query_grid = all_queries.reshape(rows_here, KV_HEADS, per_group, 2, HEAD_DIM)
    stat_shape = (KV_HEADS, per_group, 2, rows_here)
    maxima = jnp.full(stat_shape, -1e30, jnp.float32)
    key_piece = lax.all_gather(key_proj, "sp", axis=0, tiled=True)
    value_piece = lax.all_gather(value_proj, "sp", axis=0, tiled=True)
    key_count = key_piece.shape[0]
    key_grid = key_piece.reshape(key_count, KV_HEADS, 2, HEAD_DIM)
    value_grid = value_piece.reshape(key_count, KV_HEADS, VALUE_DIM)
    scores = (
        jnp.einsum("qagcd,kacd->agcqk", query_grid, key_grid, preferred_element_type=jnp.float32)
        * scaling
    )
    highest = jnp.maximum(maxima, jnp.max(scores, axis=-1))
    weights = jnp.exp(scores - highest[..., None])
    totals = jnp.sum(weights, axis=-1)
    weighted = jnp.einsum(
        "agcqk,kae->agcqe",
        weights.astype(jnp.bfloat16),
        value_grid,
        preferred_element_type=jnp.float32,
    )
    maxima, totals, weighted = (highest, totals, weighted)
    maxima = maxima.reshape(HEADS, 2, rows_here)
    totals = totals.reshape(HEADS, 2, rows_here)
    weighted = weighted.reshape(HEADS, 2, rows_here, VALUE_DIM)
    tp_size = lax.axis_size("tp")
    local_heads = HEADS // tp_size
    got_max, got_tot, got_sum = (
        lax.all_to_all(maxima, "tp", split_axis=0, concat_axis=0, tiled=True),
        lax.all_to_all(totals, "tp", split_axis=0, concat_axis=0, tiled=True),
        lax.all_to_all(weighted, "tp", split_axis=0, concat_axis=0, tiled=True),
    )
    got_max = got_max.reshape(tp_size, local_heads, 2, rows_here)
    got_tot = got_tot.reshape(tp_size, local_heads, 2, rows_here)
    got_sum = got_sum.reshape(tp_size, local_heads, 2, rows_here, VALUE_DIM)
    highest = jnp.max(got_max, axis=0)
    factor = jnp.exp(got_max - highest)
    totals_all = jnp.sum(factor * got_tot, axis=0)
    sums_all = jnp.sum(factor[..., None] * got_sum, axis=0)
    lambdas = lax.dynamic_slice_in_dim(diff_lambda, lax.axis_index("tp") * local_heads, local_heads)
    own_heads = head_norm(sums_all / totals_all[..., None], lambdas, head_gain)
    head_outputs = lax.all_gather(own_heads, "tp", axis=0, tiled=True)
    out_grid = out_weight.reshape(HEADS, VALUE_DIM, out_weight.shape[1])
    projected = jnp.einsum(
        "hqe,hed->qd", head_outputs, out_grid, preferred_element_type=jnp.float32
    )
    after_mix = residual.astype(jnp.float32) + projected
    squares = lax.psum(jnp.sum(after_mix * after_mix, axis=1), "tp")
    normed = (after_mix * lax.rsqrt(squares / D + epsilon)[:, None] * norm_gain).astype(
        jnp.bfloat16
    )
    full_rows = lax.all_gather(normed, "tp", axis=1, tiled=True)
    hidden = jnp.dot(
        full_rows,
        lax.all_gather(up_weight, "sp", axis=0, tiled=True),
        preferred_element_type=jnp.float32,
    )
    activated = jnp.square(jax.nn.relu(hidden)).astype(jnp.bfloat16)
    partial_value = jnp.dot(
        activated,
        lax.all_gather(down_weight, "sp", axis=1, tiled=True),
        preferred_element_type=jnp.float32,
    )
    mixer_sum = lax.psum_scatter(partial_value, "tp", scatter_dimension=1, tiled=True)
    return (after_mix + mixer_sum).astype(jnp.bfloat16)


MESH = pl.DeviceIdType.MESH
F32 = jnp.float32
BF16 = jnp.bfloat16
CHIP_CORES = 2
Y_CHIPS = 2
Z_CHIPS = 4
OWN, NEAR, FIRST, SECOND = range(Z_CHIPS)


class Slots:
    def __init__(self):
        self.used = 0

    def take(self, count):
        base = self.used
        self.used += count
        return base


def fused_kernel(
    residual, queries, keys, values, lambdas, head_gain, out_weight, norm_gain,
    up, down, out,
    kv_all, up_all, down_all, q_buf, res_buf, w_buf, heads_all, squares, tokens, act,
    parts, parts_in, sum_out, sum_in, after, local_sem, send_sem, recv_sem,
):
    x = lax.axis_index("tp")
    s = lax.axis_index("sp")
    core, y, z = s % CHIP_CORES, (s // CHIP_CORES) % Y_CHIPS, s // (CHIP_CORES * Y_CHIPS)

    def place(z_, y_, c_):
        return (z_ * Y_CHIPS + y_) * CHIP_CORES + c_

    half = z // 2
    inner = ((z + 1) // 2) % 2
    z_near = 4 * half + 1 - z
    z_first = Z_CHIPS - 1 - z
    z_second = 5 - 4 * half - z_first
    z_in, z_out = 2 - half, 3 - 3 * half
    is_inner, is_outer = inner == 1, inner == 0

    def in_column(z_):
        return {"sp": place(z_, y, core), "tp": x}

    mate = {"sp": s, "tp": 1 - x}
    beside = {"sp": place(z, 1 - y, core), "tp": x}
    twin = {"sp": place(z, y, 1 - core), "tp": x}
    near, across, beyond = in_column(z_near), in_column(z_in), in_column(z_out)

    barrier = pltpu.get_barrier_semaphore()
    peers = [mate, beside, twin, near, across, beyond]
    for peer in peers:
        pl.semaphore_signal(barrier, inc=1, device_id=peer, device_id_type=MESH)

    count = {"local": 0, "remote": 0}
    slots = Slots()
    started = []

    def bring(src, dst):
        copy = pltpu.make_async_copy(src, dst, local_sem.at[count["local"]])
        count["local"] += 1
        copy.start()
        return copy

    def send(src, dst, peer, slot, when=None):
        i = count["remote"]
        count["remote"] += 1

        def copy():
            return pltpu.make_async_remote_copy(
                src_ref=src, dst_ref=dst, send_sem=send_sem.at[i], recv_sem=recv_sem.at[slot],
                device_id=peer, device_id_type=MESH,
            )

        if when is None:
            copy().start()
        else:
            pl.when(when)(lambda: copy().start())
        started.append((copy, when))

    def arrive(dst, slot):
        pltpu.make_async_remote_copy(
            src_ref=dst, dst_ref=dst, send_sem=send_sem.at[0], recv_sem=recv_sem.at[slot],
            device_id=mate, device_id_type=MESH,
        ).wait_recv()

    few = keys.shape[0]
    kw = kv_all.shape[2] // 2
    chunk = up_all.shape[2]
    lanes = down.shape[1]

    def half_of(ref, part):
        return ref.at[:, pl.ds(pl.multiple_of(part * kw, kw), kw)]

    def kv_rows(block, part, side):
        return kv_all.at[block, pl.ds(pl.multiple_of(part * few, few), few), pl.ds(side * kw, kw)]

    own_kv = [bring(half_of(keys, x), kv_rows(s, x, 0)), bring(half_of(values, x), kv_rows(s, x, 1))]
    q_copy = bring(queries, q_buf)

    pl.semaphore_wait(barrier, len(peers))

    swap = slots.take(2)
    for side, ref in enumerate((keys, values)):
        send(half_of(ref, 1 - x), kv_rows(s, x, side), mate, swap + side)
    w_copy = bring(out_weight, w_buf)
    r_copy = bring(residual, res_buf)

    def up_chunk(part):
        return up.at[:, pl.ds(pl.multiple_of(part * chunk, chunk), chunk)]

    def down_chunk(part):
        return down.at[pl.ds(pl.multiple_of(part * chunk, chunk), chunk), :]

    def kv_block(b):
        return kv_all.at[b]

    def up_block(b):
        return up_all.at[b]

    def down_block(b):
        return down_all.at[:, pl.ds(pl.multiple_of(b * lanes, lanes), lanes)]

    up_own = bring(up_chunk(z), up_block(s))
    down_own = bring(down_chunk(z), down_block(s))

    def multicast(block, base):
        send(block(z), block(z), near, base)
        send(block(z), block(z), across, base + 2 - inner)

    def relay(block, base, j):
        z_ = (z_in, z_out)[j]
        send(block(z_), block(z_), near, base + 1 + j, is_inner)

    class Stream:
        def __init__(self, block_of, order):
            self.block_of, self.order = block_of, order
            self.z, self.y, self.twin, self.far = (slots.take(Z_CHIPS) for _ in range(4))

        def block(self, k, y_, c_):
            return self.block_of(place(self.order[k], y_, c_))

        def wait_z(self, k):
            arrive(self.block(k, y, core), self.z + k)

        def spread(self, k):
            b = self.block(k, y, core)
            send(b, b, beside, self.y + k)
            send(b, b, twin, self.twin + k)

        def pass_on(self, k):
            b = self.block(k, 1 - y, core)
            arrive(b, self.y + k)
            send(b, b, twin, self.far + k)

        def wait_twin(self, k):
            arrive(self.block(k, y, 1 - core), self.twin + k)
            arrive(self.block(k, 1 - y, 1 - core), self.far + k)

    kv = Stream(kv_block, (z, z_near, z_in, z_out))
    ups = Stream(up_block, (z, z_near, z_first, z_second))
    downs = Stream(down_block, (z, z_near, z_first, z_second))

    def column_kv(z_):
        return kv_block(place(z_, y, core))

    for copy in own_kv:
        copy.wait()
    for side in range(2):
        arrive(kv_rows(s, 1 - x, side), swap + side)
    multicast(column_kv, kv.z + 1)
    kv.spread(OWN)
    for k in (NEAR, FIRST, SECOND):
        z_ = ups.order[k]
        send(up_chunk(z_), up_block(s), in_column(z_), ups.z + k)
    kv.wait_z(NEAR)
    kv.spread(NEAR)
    kv.pass_on(OWN)
    kv.wait_z(2)
    relay(column_kv, kv.z + 1, 0)
    kv.spread(2)
    kv.pass_on(NEAR)
    kv.wait_z(3)
    relay(column_kv, kv.z + 1, 1)
    kv.spread(3)
    up_own.wait()
    ups.spread(OWN)
    kv.pass_on(2)
    kv.pass_on(3)
    for k in range(Z_CHIPS):
        kv.wait_twin(k)
    q_copy.wait()

    local_heads = q_buf.shape[1] // (2 * HEAD_DIM)
    blocks, per_block = kv_all.shape[0], kv_all.shape[1]
    key_count = blocks * per_block
    factor = HEAD_DIM ** (-0.5) * math.log2(math.e)
    vals = lambda: kv_all[:, :, kw:].reshape(key_count, kw)
    heads = slots.take(local_heads)

    def head_cols(part, h):
        return heads_all.at[part, :, pl.ds(h * VALUE_DIM, VALUE_DIM)]

    for h in range(local_heads):
        maps = []
        for c in range(2):
            q = q_buf[:, (2 * h + c) * HEAD_DIM : (2 * h + c + 1) * HEAD_DIM]
            k = kv_all[:, :, c * HEAD_DIM : (c + 1) * HEAD_DIM].reshape(key_count, HEAD_DIM)
            scores = lax.dot_general(q, k, (((1,), (1,)), ((), ())), preferred_element_type=F32)
            top = jnp.max(scores, axis=1, keepdims=True)
            weights = jnp.exp2((scores - top) * factor)
            total = jnp.sum(weights, axis=1, keepdims=True)
            summed = jnp.dot(weights.astype(BF16), vals(), preferred_element_type=F32)
            maps.append(summed / total)
        diff = maps[0] - lambdas[x * local_heads + h] * maps[1]
        scaled = diff * lax.rsqrt(jnp.mean(diff * diff, axis=1, keepdims=True) + epsilon)
        heads_all[x, :, pl.ds(h * VALUE_DIM, VALUE_DIM)] = (scaled * head_gain[...]).astype(BF16)
        send(head_cols(x, h), head_cols(x, h), mate, heads + h)
        if h == 0:
            ups.wait_z(NEAR)
            ups.spread(NEAR)
        if h == 1:
            ups.pass_on(OWN)
        if h == local_heads - 1:
            ups.wait_z(FIRST)
            ups.spread(FIRST)

    wide = heads_all.shape[2]
    rows = heads_all.shape[1]
    w_copy.wait()
    r_copy.wait()

    def w_rows(part):
        return w_buf[pl.ds(pl.multiple_of(part * wide, wide), wide), :]

    mix = res_buf[...].astype(F32) + jnp.dot(heads_all[x], w_rows(x), preferred_element_type=F32)
    for h in range(local_heads):
        arrive(head_cols(1 - x, h), heads + h)
    mix = mix + jnp.dot(heads_all[1 - x], w_rows(1 - x), preferred_element_type=F32)
    after[...] = mix
    own_squares = jnp.sum(mix * mix, axis=1, keepdims=True)
    squares[x] = jnp.broadcast_to(own_squares, squares.shape[1:])
    square_slot = slots.take(1)
    send(squares.at[x], squares.at[x], mate, square_slot)
    arrive(squares.at[1 - x], square_slot)
    width = 2 * wide
    mean = (own_squares + squares[1 - x][:, :1]) / width
    tokens[z, x] = (after[...] * lax.rsqrt(mean + epsilon) * norm_gain[...]).astype(BF16)

    def column_tokens(z_):
        return tokens.at[z_, x]

    token_z = slots.take(Z_CHIPS - 1)
    token_x = slots.take(Z_CHIPS)

    def cross(z_, i):
        send(column_tokens(z_), column_tokens(z_), mate, token_x + i)

    def send_down(k):
        z_ = downs.order[k]
        send(down_chunk(z_), down_block(s), in_column(z_), downs.z + k)

    multicast(column_tokens, token_z)
    cross(z, OWN)
    send_down(FIRST)
    send_down(SECOND)
    ups.wait_z(SECOND)
    ups.spread(SECOND)
    ups.pass_on(NEAR)
    arrive(column_tokens(z_near), token_z)
    cross(z_near, NEAR)
    ups.pass_on(FIRST)
    for j, z_ in enumerate((z_in, z_out)):
        arrive(column_tokens(z_), token_z + 1 + j)
        relay(column_tokens, token_z, j)
        cross(z_, 2 + j)
    send_down(NEAR)
    down_own.wait()
    downs.spread(OWN)
    ups.pass_on(SECOND)
    for k in range(Z_CHIPS):
        ups.wait_twin(k)

    halves = up_all.shape[0] // 2

    def up_rows(i):
        return up_all[i * halves : (i + 1) * halves].reshape(wide, chunk)

    def activate(pair):
        first = pl.ds(2 * pair, 2)
        hidden = jnp.dot(
            tokens[first, 0].reshape(2 * rows, wide), up_rows(0), preferred_element_type=F32
        ) + jnp.dot(
            tokens[first, 1].reshape(2 * rows, wide), up_rows(1), preferred_element_type=F32
        )
        act[first] = jnp.square(jnp.maximum(hidden, 0.0)).astype(BF16).reshape(2, rows, chunk)

    for i, z_ in enumerate((z, z_near)):
        arrive(tokens.at[z_, 1 - x], token_x + i)
    activate(half)
    downs.pass_on(OWN)
    downs.wait_z(NEAR)
    downs.spread(NEAR)
    for i, z_ in ((2, z_in), (3, z_out)):
        arrive(tokens.at[z_, 1 - x], token_x + i)
    activate(1 - half)

    span = parts.shape[3]
    early_kept, early_sent = x == half, x != half
    part_slot = slots.take(2 * Z_CHIPS)
    to_visit = (z_in, z_out, z_near, z)

    def project(group):
        cols = down_all[:, pl.ds(pl.multiple_of(group * span, span), span)]
        product = jnp.dot(act[...].reshape(Z_CHIPS * rows, chunk), cols, preferred_element_type=F32)
        parts[group] = product.astype(BF16).reshape(Z_CHIPS, rows, span)

    def hand_over(group, when):
        a = group % 2
        for z_ in to_visit:
            send(parts.at[group, z_], parts_in.at[a, z_], mate,
                 part_slot + a * Z_CHIPS + z_, when)

    sum_slot = slots.take(4 * 2)

    def both(a, z_):
        arrive(parts_in.at[a, z_], part_slot + a * Z_CHIPS + z_)
        return parts[2 * x + a, z_].astype(F32) + parts_in[a, z_].astype(F32)

    def settle_own(a, when):
        @pl.when(when)
        def _():
            cols = pl.ds(pl.multiple_of(a * span, span), span)
            after[:, cols] = after[:, cols] + both(a, z)

    def deliver(a, i, row, peer, when):
        send(sum_out.at[i, a], sum_in.at[row, a], peer, sum_slot + 2 * row + a, when)

    def settle_near(a, when):
        @pl.when(when)
        def _():
            sum_out[0, a] = both(a, z_near).astype(BF16)

        deliver(a, 0, 0, near, when)

    def settle_far(a, j, when):
        z_ = (z_in, z_out)[j]

        @pl.when(when & is_outer)
        def _():
            sum_out[1 + j, a] = both(a, z_).astype(BF16)

        deliver(a, 1 + j, 2 + j, near, when & is_outer)

        @pl.when(when & is_inner)
        def _():
            mine = both(a, z_)
            arrive(sum_in.at[2 + j, a], sum_slot + 2 * (2 + j) + a)
            sum_out[1 + j, a] = (mine + sum_in[2 + j, a].astype(F32)).astype(BF16)

        deliver(a, 1 + j, 1, (across, beyond)[j], when & is_inner)

    for k in (OWN, NEAR):
        if k == NEAR:
            downs.pass_on(NEAR)
        downs.wait_twin(k)
    for i in range(2):
        project(2 * half + i)
        hand_over(2 * half + i, early_sent)

    downs.wait_z(FIRST)
    downs.spread(FIRST)
    downs.pass_on(FIRST)
    downs.wait_twin(FIRST)
    project(z_first)
    hand_over(z_first, early_kept)
    downs.wait_z(SECOND)
    downs.spread(SECOND)
    for j in range(2):
        settle_far(0, j, early_kept)
    settle_near(0, early_kept)
    settle_own(0, early_kept)
    downs.pass_on(SECOND)
    downs.wait_twin(SECOND)
    project(z_second)
    hand_over(z_second, early_kept)
    for j in range(2):
        settle_far(1, j, early_kept)
    settle_near(1, early_kept)
    settle_own(1, early_kept)

    late_outer, late_inner = early_sent & is_outer, early_sent & is_inner
    a_first, a_second = z_first % 2, z_second % 2
    for j in range(2):
        settle_far(a_first, j, late_outer)
    settle_near(a_first, early_sent)
    settle_own(a_first, early_sent)
    for j in range(2):
        settle_far(a_second, j, early_sent)
    settle_near(a_second, early_sent)
    settle_own(a_second, early_sent)
    for j in range(2):
        settle_far(a_first, j, late_inner)

    for row in range(2):
        for a in range(2):
            arrive(sum_in.at[row, a], sum_slot + 2 * row + a)
    for a in range(2):
        cols = slice(a * span, (a + 1) * span)
        total = after[:, cols] + sum_in[0, a].astype(F32) + sum_in[1, a].astype(F32)
        out[:, cols] = total.astype(out.dtype)
    for copy, when in started:
        if when is None:
            copy().wait_send()
        else:
            pl.when(when)(lambda: copy().wait_send())


def on_chip(sp_size, residual, queries, key_proj, value_proj, diff_lambda, head_gain, out_weight,
            norm_gain, up_weight, down_weight):
    rows, wide = residual.shape
    kw = key_proj.shape[1] // KV_HEADS
    chunk = up_weight.shape[1] // Z_CHIPS
    span = sp_size // Z_CHIPS * down_weight.shape[1]
    hbm = pl.BlockSpec(memory_space=pltpu.HBM)
    vmem = pl.BlockSpec(memory_space=pltpu.VMEM)
    smem = pl.BlockSpec(memory_space=pltpu.SMEM)
    copies = 160
    return pl.pallas_call(
        fused_kernel,
        out_shape=jax.ShapeDtypeStruct(residual.shape, BF16),
        in_specs=[hbm, hbm, hbm, hbm, smem, vmem, hbm, vmem, hbm, hbm],
        out_specs=vmem,
        scratch_shapes=[
            pltpu.VMEM((sp_size, 2 * key_proj.shape[0], 2 * kw), BF16),
            pltpu.VMEM((sp_size, up_weight.shape[0], chunk), BF16),
            pltpu.VMEM((chunk, sp_size * down_weight.shape[1]), BF16),
            pltpu.VMEM(queries.shape, BF16),
            pltpu.VMEM(residual.shape, BF16),
            pltpu.VMEM(out_weight.shape, BF16),
            pltpu.VMEM((2, rows, wide), BF16),
            pltpu.VMEM((2, rows, 128), F32),
            pltpu.VMEM((Z_CHIPS, 2, rows, wide), BF16),
            pltpu.VMEM((Z_CHIPS, rows, chunk), BF16),
            pltpu.VMEM((Z_CHIPS, Z_CHIPS, rows, span), BF16),
            pltpu.VMEM((2, Z_CHIPS, rows, span), BF16),
            pltpu.VMEM((3, 2, rows, span), BF16),
            pltpu.VMEM((4, 2, rows, span), BF16),
            pltpu.VMEM((rows, wide), F32),
            pltpu.SemaphoreType.DMA((8,)),
            pltpu.SemaphoreType.DMA((copies,)),
            pltpu.SemaphoreType.DMA((copies,)),
        ],
        compiler_params=pltpu.CompilerParams(
            collective_id=0, has_side_effects=True, vmem_limit_bytes=60 * 2**20
        ),
        name="fused_layer",
    )(residual, queries, key_proj, value_proj, diff_lambda, head_gain.reshape(1, -1), out_weight,
      norm_gain.reshape(1, -1), up_weight, down_weight)


def solution(mesh):
    sp_size, tp_size = mesh.shape["sp"], mesh.shape["tp"]
    direct = tp_size == KV_HEADS == 2 and sp_size == Z_CHIPS * Y_CHIPS * CHIP_CORES
    body = functools.partial(on_chip, sp_size) if direct else on_device
    return jax.shard_map(
        body,
        mesh=mesh,
        in_specs=(
            P("sp", "tp"),
            P("sp", "tp"),
            P(("sp", "tp"), None),
            P(("sp", "tp"), None),
            P(),
            P(),
            P(None, "tp"),
            P("tp"),
            P("sp", "tp"),
            P("tp", "sp"),
        ),
        out_specs=P("sp", "tp"),
        check_vma=False,
    )
```

time: 132 us -> 139 us (1.053)
  Pallas kernels: 130 us -> 137 us
    pallas_call x1, Pallas kernels: 130 us -> 137 us  [on_chip(): pl.pallas_call(fused_kernel, out_shape=jax.ShapeDtypeStruct(residual.shap...]
where the time goes in v1:
time: 139 us
  Pallas kernels  137 us (99%)
  local copies, waits for them, and re-layouts  1.67 us (1%)
    pallas_call x1, Pallas kernels, on_chip(): pl.pallas_call(fused_kernel, out_shape=jax.ShapeDtypeStruct(residual.shap...  137 us

profile of v1, /device:TPU:0, one launch (start us, length us, event | category | flops | bytes accessed | tf_op | source)
XLA Modules:
  0.0 139.0 jit_solution(11537974287257433974)
XLA Ops:
  0.0 137.3 %fused_layer.1 = bf16[128,1024]{1,0:T(8,128)(2,1)} custom-call(bf16[128,1024]{1,0:T(8,128)(2,1)} %residual.1, bf16[128,1024]{1,0:T(8,128)(2,1)} %queries.1, bf16[64,512]{1,0:T(8,128)(2,1)} %keys.1, bf16[64,512]{1,0:T(8,128)(2,1)} %values.1, f32[8]{0:T(128)} %lambdas.1, f32[1,256]{1,0:T(1,128)} %bitcast.3, bf16[2048,1024]{1,0:T(8,128)(2,1)} %out_weight.1, ...), custom_call_target="tpu_custom_call" | custom-call | tf_op jit(solution)/shard_map/fused_layer/pallas_call | solution.py:541
  137.3 1.7 %copy.12 = bf16[128,1024]{1,0:T(8,128)(2,1)} copy(bf16[128,1024]{1,0:T(8,128)(2,1)} %fused_layer.1) | data formatting | bytes 524288

commit v2 on v1

--- a/solution.py
+++ b/solution.py
@@ -117,7 +117,7 @@
 CHIP_CORES = 2
 Y_CHIPS = 2
 Z_CHIPS = 4
-OWN, NEAR, FIRST, SECOND = range(Z_CHIPS)
+OWN, NEAR, FAR, MID = range(Z_CHIPS)
 
 
 class Slots:
@@ -146,8 +146,6 @@
     half = z // 2
     inner = ((z + 1) // 2) % 2
     z_near = 4 * half + 1 - z
-    z_first = Z_CHIPS - 1 - z
-    z_second = 5 - 4 * half - z_first
     z_in, z_out = 2 - half, 3 - 3 * half
     is_inner, is_outer = inner == 1, inner == 0
 
@@ -174,7 +172,7 @@
         copy.start()
         return copy
 
-    def send(src, dst, peer, slot, when=None):
+    def send(src, dst, peer, slot, when=None, waits=True):
         i = count["remote"]
         count["remote"] += 1
 
@@ -188,9 +186,14 @@
             copy().start()
         else:
             pl.when(when)(lambda: copy().start())
-        started.append((copy, when))
-
-    def arrive(dst, slot):
+        if waits:
+            started.append((copy, when))
+        return copy
+
+    def arrive(dst, slot, when=None):
+        if when is not None:
+            pl.when(when)(lambda: arrive(dst, slot))
+            return
         pltpu.make_async_remote_copy(
             src_ref=dst, dst_ref=dst, send_sem=send_sem.at[0], recv_sem=recv_sem.at[slot],
             device_id=mate, device_id_type=MESH,
@@ -252,13 +255,12 @@
         def block(self, k, y_, c_):
             return self.block_of(place(self.order[k], y_, c_))
 
-        def wait_z(self, k):
-            arrive(self.block(k, y, core), self.z + k)
-
-        def spread(self, k):
+        def spread(self, k, when=None):
             b = self.block(k, y, core)
-            send(b, b, beside, self.y + k)
-            send(b, b, twin, self.twin + k)
+            if k != OWN:
+                arrive(b, self.z + k, when)
+            send(b, b, beside, self.y + k, when)
+            send(b, b, twin, self.twin + k, when)
 
         def pass_on(self, k):
             b = self.block(k, 1 - y, core)
@@ -270,35 +272,52 @@
             arrive(self.block(k, 1 - y, 1 - core), self.far + k)
 
     kv = Stream(kv_block, (z, z_near, z_in, z_out))
-    ups = Stream(up_block, (z, z_near, z_first, z_second))
-    downs = Stream(down_block, (z, z_near, z_first, z_second))
+    ups = Stream(up_block, (z, z_near, z_out, z_in))
+    downs = Stream(down_block, (z, z_near, z_out, z_in))
+
+    def deal(stream, piece_of, k, when=None):
+        z_, peer, slot = {
+            NEAR: (z_near, near, NEAR), FAR: (z_out, beyond, FAR + inner), MID: (z_in, across, FAR + inner),
+        }[k]
+        send(piece_of(z_), stream.block_of(s), peer, stream.z + slot, when)
+
+    def kv_onward(k):
+        b = kv.block(k, y, core)
+        send(b, b, beside, kv.y + k)
+        send(b, b, twin, kv.twin + k)
 
     def column_kv(z_):
         return kv_block(place(z_, y, core))
 
+    outlets = (
+        (beside, kv.y), (twin, kv.twin), (near, kv.z + 1), (across, kv.z + 3 - inner)
+    )
+    for peer, slot in outlets:
+        for side, ref in enumerate((keys, values)):
+            send(half_of(ref, x), kv_rows(s, x, side), peer, slot)
+    for side in range(2):
+        arrive(kv_rows(s, 1 - x, side), swap + side)
+    mates_rows = kv_all.at[s, pl.ds(pl.multiple_of((1 - x) * few, few), few), :]
+    for peer, slot in outlets:
+        send(mates_rows, mates_rows, peer, slot)
+    deal(ups, up_chunk, NEAR, is_outer)
+    deal(ups, up_chunk, MID)
+    kv.spread(1)
+    arrive(kv.block(2, y, core), kv.z + 2)
+    relay(column_kv, kv.z + 1, 0)
+    arrive(kv.block(3, y, core), kv.z + 3, is_inner)
+    relay(column_kv, kv.z + 1, 1)
+    deal(ups, up_chunk, NEAR, is_inner)
+    kv_onward(2)
+    arrive(kv.block(3, y, core), kv.z + 3, is_outer)
+    deal(ups, up_chunk, FAR)
+    kv_onward(3)
+    up_own.wait()
+    ups.spread(OWN)
     for copy in own_kv:
         copy.wait()
-    for side in range(2):
-        arrive(kv_rows(s, 1 - x, side), swap + side)
-    multicast(column_kv, kv.z + 1)
-    kv.spread(OWN)
-    for k in (NEAR, FIRST, SECOND):
-        z_ = ups.order[k]
-        send(up_chunk(z_), up_block(s), in_column(z_), ups.z + k)
-    kv.wait_z(NEAR)
-    kv.spread(NEAR)
-    kv.pass_on(OWN)
-    kv.wait_z(2)
-    relay(column_kv, kv.z + 1, 0)
-    kv.spread(2)
-    kv.pass_on(NEAR)
-    kv.wait_z(3)
-    relay(column_kv, kv.z + 1, 1)
-    kv.spread(3)
-    up_own.wait()
-    ups.spread(OWN)
-    kv.pass_on(2)
-    kv.pass_on(3)
+    for k in range(Z_CHIPS):
+        kv.pass_on(k)
     for k in range(Z_CHIPS):
         kv.wait_twin(k)
     q_copy.wait()
@@ -328,14 +347,11 @@
         scaled = diff * lax.rsqrt(jnp.mean(diff * diff, axis=1, keepdims=True) + epsilon)
         heads_all[x, :, pl.ds(h * VALUE_DIM, VALUE_DIM)] = (scaled * head_gain[...]).astype(BF16)
         send(head_cols(x, h), head_cols(x, h), mate, heads + h)
-        if h == 0:
-            ups.wait_z(NEAR)
-            ups.spread(NEAR)
-        if h == 1:
-            ups.pass_on(OWN)
-        if h == local_heads - 1:
-            ups.wait_z(FIRST)
-            ups.spread(FIRST)
+        if h < 2:
+            ups.spread((NEAR, FAR)[h], is_inner)
+    ups.spread(MID, is_inner)
+    ups.spread(NEAR, is_outer)
+    ups.pass_on(OWN)
 
     wide = heads_all.shape[2]
     rows = heads_all.shape[1]
@@ -368,28 +384,36 @@
     def cross(z_, i):
         send(column_tokens(z_), column_tokens(z_), mate, token_x + i)
 
-    def send_down(k):
-        z_ = downs.order[k]
-        send(down_chunk(z_), down_block(s), in_column(z_), downs.z + k)
+    relayed = []
+
+    def collect(j, when):
+        z_ = (z_in, z_out)[j]
+
+        @pl.when(when)
+        def _():
+            arrive(column_tokens(z_), token_z + 1 + j)
+
+        copy = send(column_tokens(z_), column_tokens(z_), near, token_z + 1 + j, when & is_inner,
+                    when is is_outer)
+        if when is is_inner:
+            relayed.append(copy)
+        send(column_tokens(z_), column_tokens(z_), mate, token_x + 2 + j, when)
 
     multicast(column_tokens, token_z)
-    cross(z, OWN)
-    send_down(FIRST)
-    send_down(SECOND)
-    ups.wait_z(SECOND)
-    ups.spread(SECOND)
-    ups.pass_on(NEAR)
+    cross(z, 0)
+    deal(downs, down_chunk, NEAR)
+    deal(downs, down_chunk, MID)
+    ups.spread(FAR, is_outer)
+    ups.spread(MID, is_outer)
     arrive(column_tokens(z_near), token_z)
-    cross(z_near, NEAR)
-    ups.pass_on(FIRST)
-    for j, z_ in enumerate((z_in, z_out)):
-        arrive(column_tokens(z_), token_z + 1 + j)
-        relay(column_tokens, token_z, j)
-        cross(z_, 2 + j)
-    send_down(NEAR)
+    cross(z_near, 1)
+    collect(0, is_inner)
+    collect(1, is_inner)
     down_own.wait()
     downs.spread(OWN)
-    ups.pass_on(SECOND)
+    for k in (NEAR, FAR, MID):
+        ups.pass_on(k)
+    collect(0, is_outer)
     for k in range(Z_CHIPS):
         ups.wait_twin(k)
 
@@ -407,31 +431,43 @@
         )
         act[first] = jnp.square(jnp.maximum(hidden, 0.0)).astype(BF16).reshape(2, rows, chunk)
 
+    span = parts.shape[3]
+    early_kept, early_sent = x == half, x != half
+    part_slot = slots.take(2 * Z_CHIPS)
+    pairs = (half, 1 - half)
+    visits = ((z_near, z), (z_in, z_out))
+
+    def project(group, i):
+        pair = pl.ds(2 * pairs[i], 2)
+        cols = down_all[:, pl.ds(pl.multiple_of(group * span, span), span)]
+        product = jnp.dot(act[pair].reshape(2 * rows, chunk), cols, preferred_element_type=F32)
+        parts[group, pair] = product.astype(BF16).reshape(2, rows, span)
+
+    def hand_over(group, i, when):
+        a = group % 2
+        for z_ in visits[i]:
+            send(parts.at[group, z_], parts_in.at[a, z_], mate, part_slot + a * Z_CHIPS + z_, when)
+
     for i, z_ in enumerate((z, z_near)):
         arrive(tokens.at[z_, 1 - x], token_x + i)
     activate(half)
+    for copy in relayed:
+        pl.when(is_inner)(lambda: copy().wait_send())
+    deal(downs, down_chunk, FAR, is_inner)
+    downs.spread(NEAR, is_outer)
+    collect(1, is_outer)
+    deal(downs, down_chunk, FAR, is_outer)
     downs.pass_on(OWN)
-    downs.wait_z(NEAR)
-    downs.spread(NEAR)
+    downs.wait_twin(OWN)
+    project(z, 0)
+    hand_over(z, 0, early_sent)
+    for k in (NEAR, MID, FAR):
+        downs.spread(k, is_inner)
     for i, z_ in ((2, z_in), (3, z_out)):
         arrive(tokens.at[z_, 1 - x], token_x + i)
     activate(1 - half)
-
-    span = parts.shape[3]
-    early_kept, early_sent = x == half, x != half
-    part_slot = slots.take(2 * Z_CHIPS)
-    to_visit = (z_in, z_out, z_near, z)
-
-    def project(group):
-        cols = down_all[:, pl.ds(pl.multiple_of(group * span, span), span)]
-        product = jnp.dot(act[...].reshape(Z_CHIPS * rows, chunk), cols, preferred_element_type=F32)
-        parts[group] = product.astype(BF16).reshape(Z_CHIPS, rows, span)
-
-    def hand_over(group, when):
-        a = group % 2
-        for z_ in to_visit:
-            send(parts.at[group, z_], parts_in.at[a, z_], mate,
-                 part_slot + a * Z_CHIPS + z_, when)
+    project(z, 1)
+    hand_over(z, 1, early_sent)
 
     sum_slot = slots.take(4 * 2)
 
@@ -472,47 +508,33 @@
 
         deliver(a, 1 + j, 1, (across, beyond)[j], when & is_inner)
 
-    for k in (OWN, NEAR):
-        if k == NEAR:
-            downs.pass_on(NEAR)
-        downs.wait_twin(k)
-    for i in range(2):
-        project(2 * half + i)
-        hand_over(2 * half + i, early_sent)
-
-    downs.wait_z(FIRST)
-    downs.spread(FIRST)
-    downs.pass_on(FIRST)
-    downs.wait_twin(FIRST)
-    project(z_first)
-    hand_over(z_first, early_kept)
-    downs.wait_z(SECOND)
-    downs.spread(SECOND)
-    for j in range(2):
-        settle_far(0, j, early_kept)
-    settle_near(0, early_kept)
-    settle_own(0, early_kept)
-    downs.pass_on(SECOND)
-    downs.wait_twin(SECOND)
-    project(z_second)
-    hand_over(z_second, early_kept)
-    for j in range(2):
-        settle_far(1, j, early_kept)
-    settle_near(1, early_kept)
-    settle_own(1, early_kept)
-
-    late_outer, late_inner = early_sent & is_outer, early_sent & is_inner
-    a_first, a_second = z_first % 2, z_second % 2
-    for j in range(2):
-        settle_far(a_first, j, late_outer)
-    settle_near(a_first, early_sent)
-    settle_own(a_first, early_sent)
-    for j in range(2):
-        settle_far(a_second, j, early_sent)
-    settle_near(a_second, early_sent)
-    settle_own(a_second, early_sent)
-    for j in range(2):
-        settle_far(a_first, j, late_inner)
+    def settle(a, when):
+        for j in range(2):
+            settle_far(a, j, when)
+        settle_near(a, when)
+        settle_own(a, when)
+
+    downs.spread(FAR, is_outer)
+    downs.pass_on(NEAR)
+    downs.wait_twin(NEAR)
+    for i in (1, 0):
+        project(z_near, i)
+        hand_over(z_near, i, early_sent)
+    downs.spread(MID, is_outer)
+    downs.pass_on(FAR)
+    downs.wait_twin(FAR)
+    for i in (1, 0):
+        project(z_out, i)
+        hand_over(z_out, i, early_kept)
+    downs.pass_on(MID)
+    downs.wait_twin(MID)
+    for i in (1, 0):
+        project(z_in, i)
+        hand_over(z_in, i, early_kept)
+    settle(half, early_kept)
+    settle(1 - half, early_kept)
+    settle(z_out % 2, early_sent)
+    settle(z_in % 2, early_sent)
 
     for row in range(2):
         for a in range(2):

time: 139 us -> 115 us (0.83)
  Pallas kernels: 137 us -> 113 us
    pallas_call x1, Pallas kernels: 137 us -> 113 us  [on_chip(): pl.pallas_call(fused_kernel, out_shape=jax.ShapeDtypeStruct(residual.shap...]
where the time goes in v2:
time: 115 us
  Pallas kernels  113 us (98%)
  local copies, waits for them, and re-layouts  1.67 us (1%)
    pallas_call x1, Pallas kernels, on_chip(): pl.pallas_call(fused_kernel, out_shape=jax.ShapeDtypeStruct(residual.shap...  113 us

profile of v2, /device:TPU:0, one launch (start us, length us, event | category | flops | bytes accessed | tf_op | source)
XLA Modules:
  0.0 115.1 jit_solution(6607639434255859050)
XLA Ops:
  0.0 113.4 %fused_layer.1 = bf16[128,1024]{1,0:T(8,128)(2,1)} custom-call(bf16[128,1024]{1,0:T(8,128)(2,1)} %residual.1, bf16[128,1024]{1,0:T(8,128)(2,1)} %queries.1, bf16[64,512]{1,0:T(8,128)(2,1)} %keys.1, bf16[64,512]{1,0:T(8,128)(2,1)} %values.1, f32[8]{0:T(128)} %lambdas.1, f32[1,256]{1,0:T(1,128)} %bitcast.3, bf16[2048,1024]{1,0:T(8,128)(2,1)} %out_weight.1, ...), custom_call_target="tpu_custom_call" | custom-call | tf_op jit(solution)/shard_map/fused_layer/pallas_call | solution.py:563
  113.4 1.7 %copy.12 = bf16[128,1024]{1,0:T(8,128)(2,1)} copy(bf16[128,1024]{1,0:T(8,128)(2,1)} %fused_layer.1) | data formatting | bytes 524288

commit v3 on v2

--- a/solution.py
+++ b/solution.py
@@ -148,6 +148,8 @@
     z_near = 4 * half + 1 - z
     z_in, z_out = 2 - half, 3 - 3 * half
     is_inner, is_outer = inner == 1, inner == 0
+    same = 1 - (x + half) % 2
+    sends_far, keeps_far = same == 1, same == 0
 
     def in_column(z_):
         return {"sp": place(z_, y, core), "tp": x}
@@ -239,17 +241,13 @@
     up_own = bring(up_chunk(z), up_block(s))
     down_own = bring(down_chunk(z), down_block(s))
 
-    def multicast(block, base):
-        send(block(z), block(z), near, base)
-        send(block(z), block(z), across, base + 2 - inner)
-
     def relay(block, base, j):
         z_ = (z_in, z_out)[j]
         send(block(z_), block(z_), near, base + 1 + j, is_inner)
 
     class Stream:
         def __init__(self, block_of, order):
-            self.block_of, self.order = block_of, order
+            self.block_of, self.order = block_of, list(order)
             self.z, self.y, self.twin, self.far = (slots.take(Z_CHIPS) for _ in range(4))
 
         def block(self, k, y_, c_):
@@ -267,18 +265,28 @@
             arrive(b, self.y + k)
             send(b, b, twin, self.far + k)
 
-        def wait_twin(self, k):
-            arrive(self.block(k, y, 1 - core), self.twin + k)
-            arrive(self.block(k, 1 - y, 1 - core), self.far + k)
+        def wait_twin(self, k, side=None):
+            if side != 1:
+                arrive(self.block(k, y, 1 - core), self.twin + k)
+            if side != 0:
+                arrive(self.block(k, 1 - y, 1 - core), self.far + k)
 
     kv = Stream(kv_block, (z, z_near, z_in, z_out))
     ups = Stream(up_block, (z, z_near, z_out, z_in))
-    downs = Stream(down_block, (z, z_near, z_out, z_in))
+    downs = Stream(down_block, (
+        z,
+        same * z_out + (1 - same) * z_near,
+        same * z_in + (1 - same) * z_out,
+        same * z_near + (1 - same) * z_in,
+    ))
 
     def deal(stream, piece_of, k, when=None):
         z_, peer, slot = {
             NEAR: (z_near, near, NEAR), FAR: (z_out, beyond, FAR + inner), MID: (z_in, across, FAR + inner),
         }[k]
+        if stream is downs:
+            theirs = same if k == NEAR else 1 - same
+            slot = 1 + (slot - 1 + 2 * theirs) % 3
         send(piece_of(z_), stream.block_of(s), peer, stream.z + slot, when)
 
     def kv_onward(k):
@@ -367,48 +375,44 @@
     mix = mix + jnp.dot(heads_all[1 - x], w_rows(1 - x), preferred_element_type=F32)
     after[...] = mix
     own_squares = jnp.sum(mix * mix, axis=1, keepdims=True)
-    squares[x] = jnp.broadcast_to(own_squares, squares.shape[1:])
-    square_slot = slots.take(1)
-    send(squares.at[x], squares.at[x], mate, square_slot)
-    arrive(squares.at[1 - x], square_slot)
     width = 2 * wide
-    mean = (own_squares + squares[1 - x][:, :1]) / width
-    tokens[z, x] = (after[...] * lax.rsqrt(mean + epsilon) * norm_gain[...]).astype(BF16)
-
-    def column_tokens(z_):
-        return tokens.at[z_, x]
-
-    token_z = slots.take(Z_CHIPS - 1)
-    token_x = slots.take(Z_CHIPS)
-
-    def cross(z_, i):
-        send(column_tokens(z_), column_tokens(z_), mate, token_x + i)
+    tokens[z, x] = (mix * norm_gain[...]).astype(BF16)
+    squares[z, x] = jnp.broadcast_to(own_squares, (rows, rows)).T[: squares.shape[2]]
+
+    token_z = slots.take(2 * (Z_CHIPS - 1))
+    token_x = slots.take(2 * Z_CHIPS)
+
+    def send_tokens(z_, peer, slot, when=None, waits=True):
+        return [
+            send(ref.at[z_, x], ref.at[z_, x], peer, slot + n, when, waits)
+            for n, ref in enumerate((tokens, squares))
+        ]
+
+    def take_tokens(z_, part, slot, when=None):
+        for n, ref in enumerate((tokens, squares)):
+            arrive(ref.at[z_, part], slot + n, when)
 
     relayed = []
 
     def collect(j, when):
         z_ = (z_in, z_out)[j]
-
-        @pl.when(when)
-        def _():
-            arrive(column_tokens(z_), token_z + 1 + j)
-
-        copy = send(column_tokens(z_), column_tokens(z_), near, token_z + 1 + j, when & is_inner,
-                    when is is_outer)
+        take_tokens(z_, x, token_z + 2 + 2 * j, when)
         if when is is_inner:
-            relayed.append(copy)
-        send(column_tokens(z_), column_tokens(z_), mate, token_x + 2 + j, when)
-
-    multicast(column_tokens, token_z)
-    cross(z, 0)
-    deal(downs, down_chunk, NEAR)
+            relayed.extend(send_tokens(z_, near, token_z + 2 + 2 * j, when, False))
+        send_tokens(z_, mate, token_x + 4 + 2 * j, when)
+
+    send_tokens(z, near, token_z)
+    send_tokens(z, across, token_z + 4 - 2 * inner)
+    send_tokens(z, mate, token_x)
+    deal(downs, down_chunk, NEAR, is_outer | keeps_far)
     deal(downs, down_chunk, MID)
     ups.spread(FAR, is_outer)
     ups.spread(MID, is_outer)
-    arrive(column_tokens(z_near), token_z)
-    cross(z_near, 1)
+    take_tokens(z_near, x, token_z)
+    send_tokens(z_near, mate, token_x + 2)
     collect(0, is_inner)
     collect(1, is_inner)
+    deal(downs, down_chunk, NEAR, is_inner & sends_far)
     down_own.wait()
     downs.spread(OWN)
     for k in (NEAR, FAR, MID):
@@ -429,119 +433,143 @@
         ) + jnp.dot(
             tokens[first, 1].reshape(2 * rows, wide), up_rows(1), preferred_element_type=F32
         )
+        factors = []
+        for i in range(2):
+            mean = (squares[2 * pair + i, 0] + squares[2 * pair + i, 1])[:1] / width
+            factors.append(jnp.broadcast_to(lax.rsqrt(mean + epsilon), (rows, rows)).T[:, :1])
+        hidden = hidden * jnp.concatenate(factors, axis=0)
         act[first] = jnp.square(jnp.maximum(hidden, 0.0)).astype(BF16).reshape(2, rows, chunk)
 
     span = parts.shape[3]
-    early_kept, early_sent = x == half, x != half
     part_slot = slots.take(2 * Z_CHIPS)
-    pairs = (half, 1 - half)
-    visits = ((z_near, z), (z_in, z_out))
-
-    def project(group, i):
-        pair = pl.ds(2 * pairs[i], 2)
-        cols = down_all[:, pl.ds(pl.multiple_of(group * span, span), span)]
-        product = jnp.dot(act[pair].reshape(2 * rows, chunk), cols, preferred_element_type=F32)
-        parts[group, pair] = product.astype(BF16).reshape(2, rows, span)
-
-    def hand_over(group, i, when):
-        a = group % 2
-        for z_ in visits[i]:
-            send(parts.at[group, z_], parts_in.at[a, z_], mate, part_slot + a * Z_CHIPS + z_, when)
+    pairs = (pl.ds(2 * half, 2), pl.ds(2 * (1 - half), 2))
+    sides = (y, 1 - y)
+
+    def project(k, side, i, when=None):
+        unit = Y_CHIPS * downs.order[k] + sides[side]
+        cols = down_all[:, pl.ds(pl.multiple_of(unit * span, span), span)]
+        product = jnp.dot(
+            act[pairs[i]].reshape(2 * rows, chunk), cols, preferred_element_type=F32
+        )
+        parts[unit, pairs[i]] = product.astype(BF16).reshape(2, rows, span)
+        if when is not False:
+            kept = unit % Z_CHIPS
+            send(parts.at[unit, pairs[i]], parts_in.at[kept, pairs[i]], mate,
+                 part_slot + 2 * kept + i, when)
 
     for i, z_ in enumerate((z, z_near)):
-        arrive(tokens.at[z_, 1 - x], token_x + i)
+        take_tokens(z_, 1 - x, token_x + 2 * i)
     activate(half)
     for copy in relayed:
         pl.when(is_inner)(lambda: copy().wait_send())
     deal(downs, down_chunk, FAR, is_inner)
-    downs.spread(NEAR, is_outer)
+    downs.wait_twin(OWN, 0)
+    project(OWN, 0, 0, keeps_far)
+    downs.spread(1, is_inner | keeps_far)
     collect(1, is_outer)
     deal(downs, down_chunk, FAR, is_outer)
     downs.pass_on(OWN)
-    downs.wait_twin(OWN)
-    project(z, 0)
-    hand_over(z, 0, early_sent)
-    for k in (NEAR, MID, FAR):
-        downs.spread(k, is_inner)
+    downs.wait_twin(OWN, 1)
+    project(OWN, 1, 0, keeps_far)
+    downs.spread(2, is_inner)
+    downs.spread(3, is_inner)
+    downs.spread(1, is_outer & sends_far)
+    downs.wait_twin(1, 0)
+    project(1, 0, 0)
     for i, z_ in ((2, z_in), (3, z_out)):
-        arrive(tokens.at[z_, 1 - x], token_x + i)
+        take_tokens(z_, 1 - x, token_x + 2 * i)
     activate(1 - half)
-    project(z, 1)
-    hand_over(z, 1, early_sent)
-
-    sum_slot = slots.take(4 * 2)
-
-    def both(a, z_):
-        arrive(parts_in.at[a, z_], part_slot + a * Z_CHIPS + z_)
-        return parts[2 * x + a, z_].astype(F32) + parts_in[a, z_].astype(F32)
-
-    def settle_own(a, when):
+    for side in range(2):
+        project(OWN, side, 1, keeps_far)
+    project(1, 0, 1)
+    downs.spread(2, is_outer)
+    downs.pass_on(1)
+    downs.wait_twin(1, 1)
+    for i in (1, 0):
+        project(1, 1, i)
+    downs.wait_twin(2, 0)
+    for i in (1, 0):
+        project(2, 0, i, sends_far)
+    downs.spread(3, is_outer)
+    downs.pass_on(2)
+    downs.wait_twin(2, 1)
+    for i in (1, 0):
+        project(2, 1, i, sends_far)
+
+    sum_slot = slots.take(4 * Z_CHIPS)
+
+    def deliver(i, u, row, peer, when):
+        send(sum_out.at[i, u], sum_in.at[row, u], peer, sum_slot + Z_CHIPS * row + u, when)
+
+    def both(u, z_):
+        return parts[Z_CHIPS * x + u, z_].astype(F32) + parts_in[u, z_].astype(F32)
+
+    def settle_far(u, when):
+        arrive(parts_in.at[u, pairs[1]], part_slot + 2 * u + 1, when)
+        for j, z_ in enumerate((z_in, z_out)):
+
+            @pl.when(when & is_outer)
+            def _():
+                sum_out[1 + j, u] = both(u, z_).astype(BF16)
+
+            deliver(1 + j, u, 2 + j, near, when & is_outer)
+
+            @pl.when(when & is_inner)
+            def _():
+                mine = both(u, z_)
+                arrive(sum_in.at[2 + j, u], sum_slot + Z_CHIPS * (2 + j) + u)
+                sum_out[1 + j, u] = (mine + sum_in[2 + j, u].astype(F32)).astype(BF16)
+
+            deliver(1 + j, u, 1, (across, beyond)[j], when & is_inner)
+
+    def settle_half(u, when):
+        arrive(parts_in.at[u, pairs[0]], part_slot + 2 * u, when)
+
         @pl.when(when)
         def _():
-            cols = pl.ds(pl.multiple_of(a * span, span), span)
-            after[:, cols] = after[:, cols] + both(a, z)
-
-    def deliver(a, i, row, peer, when):
-        send(sum_out.at[i, a], sum_in.at[row, a], peer, sum_slot + 2 * row + a, when)
-
-    def settle_near(a, when):
+            sum_out[0, u] = both(u, z_near).astype(BF16)
+
+        deliver(0, u, 0, near, when)
+
         @pl.when(when)
         def _():
-            sum_out[0, a] = both(a, z_near).astype(BF16)
-
-        deliver(a, 0, 0, near, when)
-
-    def settle_far(a, j, when):
-        z_ = (z_in, z_out)[j]
-
-        @pl.when(when & is_outer)
-        def _():
-            sum_out[1 + j, a] = both(a, z_).astype(BF16)
-
-        deliver(a, 1 + j, 2 + j, near, when & is_outer)
-
-        @pl.when(when & is_inner)
-        def _():
-            mine = both(a, z_)
-            arrive(sum_in.at[2 + j, a], sum_slot + 2 * (2 + j) + a)
-            sum_out[1 + j, a] = (mine + sum_in[2 + j, a].astype(F32)).astype(BF16)
-
-        deliver(a, 1 + j, 1, (across, beyond)[j], when & is_inner)
-
-    def settle(a, when):
-        for j in range(2):
-            settle_far(a, j, when)
-        settle_near(a, when)
-        settle_own(a, when)
-
-    downs.spread(FAR, is_outer)
-    downs.pass_on(NEAR)
-    downs.wait_twin(NEAR)
+            cols = pl.ds(pl.multiple_of(u * span, span), span)
+            after[:, cols] = after[:, cols] + both(u, z)
+
+    def columns(a):
+        return [Y_CHIPS * a + side for side in sides]
+
+    outer_sends, inner_sends = sends_far & is_outer, sends_far & is_inner
+    for u in columns(half):
+        settle_far(u, outer_sends)
+    downs.wait_twin(3, 0)
     for i in (1, 0):
-        project(z_near, i)
-        hand_over(z_near, i, early_sent)
-    downs.spread(MID, is_outer)
-    downs.pass_on(FAR)
-    downs.wait_twin(FAR)
+        project(3, 0, i, False)
+    downs.pass_on(3)
+    downs.wait_twin(3, 1)
     for i in (1, 0):
-        project(z_out, i)
-        hand_over(z_out, i, early_kept)
-    downs.pass_on(MID)
-    downs.wait_twin(MID)
-    for i in (1, 0):
-        project(z_in, i)
-        hand_over(z_in, i, early_kept)
-    settle(half, early_kept)
-    settle(1 - half, early_kept)
-    settle(z_out % 2, early_sent)
-    settle(z_in % 2, early_sent)
+        project(3, 1, i, False)
+    for u in columns(1 - half):
+        settle_far(u, outer_sends)
+        settle_half(u, inner_sends)
+    for u in columns(half):
+        settle_half(u, outer_sends)
+        settle_far(u, inner_sends)
+        settle_half(u, inner_sends)
+    for u in columns(1 - half):
+        settle_half(u, outer_sends)
+        settle_far(u, inner_sends)
+    for u in columns(z_out % 2) + columns(z_in % 2):
+        settle_far(u, keeps_far & is_outer)
+        settle_half(u, keeps_far)
+        settle_far(u, keeps_far & is_inner)
 
     for row in range(2):
-        for a in range(2):
-            arrive(sum_in.at[row, a], sum_slot + 2 * row + a)
-    for a in range(2):
-        cols = slice(a * span, (a + 1) * span)
-        total = after[:, cols] + sum_in[0, a].astype(F32) + sum_in[1, a].astype(F32)
+        for u in range(Z_CHIPS):
+            arrive(sum_in.at[row, u], sum_slot + Z_CHIPS * row + u)
+    for u in range(Z_CHIPS):
+        cols = slice(u * span, (u + 1) * span)
+        total = after[:, cols] + sum_in[0, u].astype(F32) + sum_in[1, u].astype(F32)
         out[:, cols] = total.astype(out.dtype)
     for copy, when in started:
         if when is None:
@@ -555,11 +583,12 @@
     rows, wide = residual.shape
     kw = key_proj.shape[1] // KV_HEADS
     chunk = up_weight.shape[1] // Z_CHIPS
-    span = sp_size // Z_CHIPS * down_weight.shape[1]
+    span = CHIP_CORES * down_weight.shape[1]
+    units = Z_CHIPS * Y_CHIPS
     hbm = pl.BlockSpec(memory_space=pltpu.HBM)
     vmem = pl.BlockSpec(memory_space=pltpu.VMEM)
     smem = pl.BlockSpec(memory_space=pltpu.SMEM)
-    copies = 160
+    copies = 256
     return pl.pallas_call(
         fused_kernel,
         out_shape=jax.ShapeDtypeStruct(residual.shape, BF16),
@@ -573,13 +602,13 @@
             pltpu.VMEM(residual.shape, BF16),
             pltpu.VMEM(out_weight.shape, BF16),
             pltpu.VMEM((2, rows, wide), BF16),
-            pltpu.VMEM((2, rows, 128), F32),
+            pltpu.VMEM((Z_CHIPS, 2, 8, rows), F32),
             pltpu.VMEM((Z_CHIPS, 2, rows, wide), BF16),
             pltpu.VMEM((Z_CHIPS, rows, chunk), BF16),
-            pltpu.VMEM((Z_CHIPS, Z_CHIPS, rows, span), BF16),
-            pltpu.VMEM((2, Z_CHIPS, rows, span), BF16),
-            pltpu.VMEM((3, 2, rows, span), BF16),
-            pltpu.VMEM((4, 2, rows, span), BF16),
+            pltpu.VMEM((units, Z_CHIPS, rows, span), BF16),
+            pltpu.VMEM((units // 2, Z_CHIPS, rows, span), BF16),
+            pltpu.VMEM((3, units // 2, rows, span), BF16),
+            pltpu.VMEM((4, units // 2, rows, span), BF16),
             pltpu.VMEM((rows, wide), F32),
             pltpu.SemaphoreType.DMA((8,)),
             pltpu.SemaphoreType.DMA((copies,)),

time: 115 us -> 111 us (0.965)
  Pallas kernels: 113 us -> 110 us
    pallas_call x1, Pallas kernels: 113 us -> 110 us  [on_chip(): pl.pallas_call(fused_kernel, out_shape=jax.ShapeDtypeStruct(residual.shap...]
where the time goes in v3:
time: 111 us
  Pallas kernels  110 us (99%)
  local copies, waits for them, and re-layouts  1.67 us (2%)
    pallas_call x1, Pallas kernels, on_chip(): pl.pallas_call(fused_kernel, out_shape=jax.ShapeDtypeStruct(residual.shap...  110 us

profile of v3, /device:TPU:0, one launch (start us, length us, event | category | flops | bytes accessed | tf_op | source)
XLA Modules:
  0.0 111.3 jit_solution(5328769713814633578)
XLA Ops:
  0.0 109.6 %fused_layer.1 = bf16[128,1024]{1,0:T(8,128)(2,1)} custom-call(bf16[128,1024]{1,0:T(8,128)(2,1)} %residual.1, bf16[128,1024]{1,0:T(8,128)(2,1)} %queries.1, bf16[64,512]{1,0:T(8,128)(2,1)} %keys.1, bf16[64,512]{1,0:T(8,128)(2,1)} %values.1, f32[8]{0:T(128)} %lambdas.1, f32[1,256]{1,0:T(1,128)} %bitcast.3, bf16[2048,1024]{1,0:T(8,128)(2,1)} %out_weight.1, ...), custom_call_target="tpu_custom_call" | custom-call | tf_op jit(solution)/shard_map/fused_layer/pallas_call | solution.py:592
  109.6 1.7 %copy.12 = bf16[128,1024]{1,0:T(8,128)(2,1)} copy(bf16[128,1024]{1,0:T(8,128)(2,1)} %fused_layer.1) | data formatting | bytes 524288

commit v4 on v3

--- a/solution.py
+++ b/solution.py
@@ -164,33 +164,41 @@
     for peer in peers:
         pl.semaphore_signal(barrier, inc=1, device_id=peer, device_id_type=MESH)
 
-    count = {"local": 0, "remote": 0}
+    local_copies = []
     slots = Slots()
-    started = []
+    outgoing = {}
 
     def bring(src, dst):
-        copy = pltpu.make_async_copy(src, dst, local_sem.at[count["local"]])
-        count["local"] += 1
+        copy = pltpu.make_async_copy(src, dst, local_sem.at[len(local_copies)])
+        local_copies.append(copy)
         copy.start()
         return copy
 
-    def send(src, dst, peer, slot, when=None, waits=True):
-        i = count["remote"]
-        count["remote"] += 1
-
-        def copy():
-            return pltpu.make_async_remote_copy(
+    def send(src, dst, peer, slot, group, when=None):
+        i = outgoing.setdefault(group, len(outgoing))
+
+        def start():
+            pltpu.make_async_remote_copy(
                 src_ref=src, dst_ref=dst, send_sem=send_sem.at[i], recv_sem=recv_sem.at[slot],
                 device_id=peer, device_id_type=MESH,
-            )
+            ).start()
 
         if when is None:
-            copy().start()
+            start()
         else:
-            pl.when(when)(lambda: copy().start())
-        if waits:
-            started.append((copy, when))
-        return copy
+            pl.when(when)(start)
+
+    def sent(group, whole, when=None):
+        def wait():
+            pltpu.make_async_remote_copy(
+                src_ref=whole, dst_ref=whole, send_sem=send_sem.at[outgoing[group]],
+                recv_sem=recv_sem.at[0], device_id=mate, device_id_type=MESH,
+            ).wait_send()
+
+        if when is None:
+            wait()
+        else:
+            pl.when(when)(wait)
 
     def arrive(dst, slot, when=None):
         if when is not None:
@@ -217,9 +225,9 @@
 
     pl.semaphore_wait(barrier, len(peers))
 
-    swap = slots.take(2)
+    swap = slots.take(1)
     for side, ref in enumerate((keys, values)):
-        send(half_of(ref, 1 - x), kv_rows(s, x, side), mate, swap + side)
+        send(half_of(ref, 1 - x), kv_rows(s, x, side), mate, swap, "swap")
     w_copy = bring(out_weight, w_buf)
     r_copy = bring(residual, res_buf)
 
@@ -243,12 +251,15 @@
 
     def relay(block, base, j):
         z_ = (z_in, z_out)[j]
-        send(block(z_), block(z_), near, base + 1 + j, is_inner)
+        send(block(z_), block(z_), near, base + 1 + j, "kv_relay", is_inner)
 
     class Stream:
-        def __init__(self, block_of, order):
-            self.block_of, self.order = block_of, list(order)
-            self.z, self.y, self.twin, self.far = (slots.take(Z_CHIPS) for _ in range(4))
+        def __init__(self, name, block_of, order, staged=False):
+            self.name, self.block_of, self.order = name, block_of, order
+            self.z, self.y = slots.take(Z_CHIPS), slots.take(Z_CHIPS)
+            self.step = int(staged)
+            self.twin = slots.take(2 * Z_CHIPS if staged else 1)
+            self.far = self.twin + Z_CHIPS * self.step
 
         def block(self, k, y_, c_):
             return self.block_of(place(self.order[k], y_, c_))
@@ -257,13 +268,13 @@
             b = self.block(k, y, core)
             if k != OWN:
                 arrive(b, self.z + k, when)
-            send(b, b, beside, self.y + k, when)
-            send(b, b, twin, self.twin + k, when)
+            send(b, b, beside, self.y + k, self.name, when)
+            send(b, b, twin, self.twin + k * self.step, self.name, when)
 
         def pass_on(self, k):
             b = self.block(k, 1 - y, core)
             arrive(b, self.y + k)
-            send(b, b, twin, self.far + k)
+            send(b, b, twin, self.far + k * self.step, self.name)
 
         def wait_twin(self, k, side=None):
             if side != 1:
@@ -271,14 +282,14 @@
             if side != 0:
                 arrive(self.block(k, 1 - y, 1 - core), self.far + k)
 
-    kv = Stream(kv_block, (z, z_near, z_in, z_out))
-    ups = Stream(up_block, (z, z_near, z_out, z_in))
-    downs = Stream(down_block, (
+    kv = Stream("kv", kv_block, (z, z_near, z_in, z_out))
+    ups = Stream("up", up_block, (z, z_near, z_out, z_in))
+    downs = Stream("down", down_block, (
         z,
         same * z_out + (1 - same) * z_near,
         same * z_in + (1 - same) * z_out,
         same * z_near + (1 - same) * z_in,
-    ))
+    ), staged=True)
 
     def deal(stream, piece_of, k, when=None):
         z_, peer, slot = {
@@ -287,12 +298,12 @@
         if stream is downs:
             theirs = same if k == NEAR else 1 - same
             slot = 1 + (slot - 1 + 2 * theirs) % 3
-        send(piece_of(z_), stream.block_of(s), peer, stream.z + slot, when)
+        send(piece_of(z_), stream.block_of(s), peer, stream.z + slot, stream.name, when)
 
     def kv_onward(k):
         b = kv.block(k, y, core)
-        send(b, b, beside, kv.y + k)
-        send(b, b, twin, kv.twin + k)
+        send(b, b, beside, kv.y + k, "kv")
+        send(b, b, twin, kv.twin, "kv")
 
     def column_kv(z_):
         return kv_block(place(z_, y, core))
@@ -302,12 +313,11 @@
     )
     for peer, slot in outlets:
         for side, ref in enumerate((keys, values)):
-            send(half_of(ref, x), kv_rows(s, x, side), peer, slot)
-    for side in range(2):
-        arrive(kv_rows(s, 1 - x, side), swap + side)
+            send(half_of(ref, x), kv_rows(s, x, side), peer, slot, "kv")
     mates_rows = kv_all.at[s, pl.ds(pl.multiple_of((1 - x) * few, few), few), :]
+    arrive(mates_rows, swap)
     for peer, slot in outlets:
-        send(mates_rows, mates_rows, peer, slot)
+        send(mates_rows, mates_rows, peer, slot, "kv")
     deal(ups, up_chunk, NEAR, is_outer)
     deal(ups, up_chunk, MID)
     kv.spread(1)
@@ -326,8 +336,7 @@
         copy.wait()
     for k in range(Z_CHIPS):
         kv.pass_on(k)
-    for k in range(Z_CHIPS):
-        kv.wait_twin(k)
+    arrive(kv_all.at[pl.ds(0, 2 * Z_CHIPS)], kv.twin)
     q_copy.wait()
 
     local_heads = q_buf.shape[1] // (2 * HEAD_DIM)
@@ -335,7 +344,7 @@
     key_count = blocks * per_block
     factor = HEAD_DIM ** (-0.5) * math.log2(math.e)
     vals = lambda: kv_all[:, :, kw:].reshape(key_count, kw)
-    heads = slots.take(local_heads)
+    heads = slots.take(1)
 
     def head_cols(part, h):
         return heads_all.at[part, :, pl.ds(h * VALUE_DIM, VALUE_DIM)]
@@ -354,7 +363,7 @@
         diff = maps[0] - lambdas[x * local_heads + h] * maps[1]
         scaled = diff * lax.rsqrt(jnp.mean(diff * diff, axis=1, keepdims=True) + epsilon)
         heads_all[x, :, pl.ds(h * VALUE_DIM, VALUE_DIM)] = (scaled * head_gain[...]).astype(BF16)
-        send(head_cols(x, h), head_cols(x, h), mate, heads + h)
+        send(head_cols(x, h), head_cols(x, h), mate, heads, "heads")
         if h < 2:
             ups.spread((NEAR, FAR)[h], is_inner)
     ups.spread(MID, is_inner)
@@ -370,8 +379,7 @@
         return w_buf[pl.ds(pl.multiple_of(part * wide, wide), wide), :]
 
     mix = res_buf[...].astype(F32) + jnp.dot(heads_all[x], w_rows(x), preferred_element_type=F32)
-    for h in range(local_heads):
-        arrive(head_cols(1 - x, h), heads + h)
+    arrive(heads_all.at[1 - x], heads)
     mix = mix + jnp.dot(heads_all[1 - x], w_rows(1 - x), preferred_element_type=F32)
     after[...] = mix
     own_squares = jnp.sum(mix * mix, axis=1, keepdims=True)
@@ -382,23 +390,19 @@
     token_z = slots.take(2 * (Z_CHIPS - 1))
     token_x = slots.take(2 * Z_CHIPS)
 
-    def send_tokens(z_, peer, slot, when=None, waits=True):
-        return [
-            send(ref.at[z_, x], ref.at[z_, x], peer, slot + n, when, waits)
-            for n, ref in enumerate((tokens, squares))
-        ]
+    def send_tokens(z_, peer, slot, when=None, group="token"):
+        for n, ref in enumerate((tokens, squares)):
+            send(ref.at[z_, x], ref.at[z_, x], peer, slot + n, (group, n), when)
 
     def take_tokens(z_, part, slot, when=None):
         for n, ref in enumerate((tokens, squares)):
             arrive(ref.at[z_, part], slot + n, when)
-
-    relayed = []
 
     def collect(j, when):
         z_ = (z_in, z_out)[j]
         take_tokens(z_, x, token_z + 2 + 2 * j, when)
         if when is is_inner:
-            relayed.extend(send_tokens(z_, near, token_z + 2 + 2 * j, when, False))
+            send_tokens(z_, near, token_z + 2 + 2 * j, when, "relay")
         send_tokens(z_, mate, token_x + 4 + 2 * j, when)
 
     send_tokens(z, near, token_z)
@@ -408,18 +412,18 @@
     deal(downs, down_chunk, MID)
     ups.spread(FAR, is_outer)
     ups.spread(MID, is_outer)
+    down_own.wait()
+    downs.spread(OWN)
     take_tokens(z_near, x, token_z)
     send_tokens(z_near, mate, token_x + 2)
     collect(0, is_inner)
     collect(1, is_inner)
     deal(downs, down_chunk, NEAR, is_inner & sends_far)
-    down_own.wait()
-    downs.spread(OWN)
     for k in (NEAR, FAR, MID):
         ups.pass_on(k)
     collect(0, is_outer)
-    for k in range(Z_CHIPS):
-        ups.wait_twin(k)
+    deal(downs, down_chunk, FAR, is_outer)
+    arrive(up_all.at[pl.ds(0, 2 * Z_CHIPS)], ups.twin)
 
     halves = up_all.shape[0] // 2
 
@@ -455,19 +459,18 @@
         if when is not False:
             kept = unit % Z_CHIPS
             send(parts.at[unit, pairs[i]], parts_in.at[kept, pairs[i]], mate,
-                 part_slot + 2 * kept + i, when)
+                 part_slot + 2 * kept + i, "parts", when)
 
     for i, z_ in enumerate((z, z_near)):
         take_tokens(z_, 1 - x, token_x + 2 * i)
     activate(half)
-    for copy in relayed:
-        pl.when(is_inner)(lambda: copy().wait_send())
+    sent(("relay", 0), tokens.at[0], is_inner)
+    sent(("relay", 1), squares.at[0], is_inner)
     deal(downs, down_chunk, FAR, is_inner)
     downs.wait_twin(OWN, 0)
     project(OWN, 0, 0, keeps_far)
     downs.spread(1, is_inner | keeps_far)
     collect(1, is_outer)
-    deal(downs, down_chunk, FAR, is_outer)
     downs.pass_on(OWN)
     downs.wait_twin(OWN, 1)
     project(OWN, 1, 0, keeps_far)
@@ -496,10 +499,11 @@
     for i in (1, 0):
         project(2, 1, i, sends_far)
 
-    sum_slot = slots.take(4 * Z_CHIPS)
+    sum_slot, pass_slot = slots.take(2), slots.take(2 * Z_CHIPS)
 
     def deliver(i, u, row, peer, when):
-        send(sum_out.at[i, u], sum_in.at[row, u], peer, sum_slot + Z_CHIPS * row + u, when)
+        slot = sum_slot + row if row < 2 else pass_slot + Z_CHIPS * (row - 2) + u
+        send(sum_out.at[i, u], sum_in.at[row, u], peer, slot, "sums", when)
 
     def both(u, z_):
         return parts[Z_CHIPS * x + u, z_].astype(F32) + parts_in[u, z_].astype(F32)
@@ -517,7 +521,7 @@
             @pl.when(when & is_inner)
             def _():
                 mine = both(u, z_)
-                arrive(sum_in.at[2 + j, u], sum_slot + Z_CHIPS * (2 + j) + u)
+                arrive(sum_in.at[2 + j, u], pass_slot + Z_CHIPS * j + u)
                 sum_out[1 + j, u] = (mine + sum_in[2 + j, u].astype(F32)).astype(BF16)
 
             deliver(1 + j, u, 1, (across, beyond)[j], when & is_inner)
@@ -564,18 +568,26 @@
         settle_half(u, keeps_far)
         settle_far(u, keeps_far & is_inner)
 
+    for group, whole in (
+        ("swap", kv_all.at[0, pl.ds(0, few), :]),
+        ("kv", kv_all.at[pl.ds(0, 3 * Z_CHIPS + 2)]),
+        ("up", up_all.at[pl.ds(0, 4 * Z_CHIPS - 1)]),
+        ("down", down_all.at[:, pl.ds(0, (4 * Z_CHIPS - 1) * lanes)]),
+        ("heads", heads_all.at[0]),
+        (("token", 0), tokens.at[pl.ds(0, 3)]),
+        (("token", 1), squares.at[pl.ds(0, 3)]),
+        ("parts", parts.at[pl.ds(0, Z_CHIPS)]),
+    ):
+        sent(group, whole)
+    sent("kv_relay", kv_all.at[pl.ds(0, 2)], is_inner)
     for row in range(2):
-        for u in range(Z_CHIPS):
-            arrive(sum_in.at[row, u], sum_slot + Z_CHIPS * row + u)
+        arrive(sum_in.at[row], sum_slot + row)
     for u in range(Z_CHIPS):
         cols = slice(u * span, (u + 1) * span)
         total = after[:, cols] + sum_in[0, u].astype(F32) + sum_in[1, u].astype(F32)
         out[:, cols] = total.astype(out.dtype)
-    for copy, when in started:
-        if when is None:
-            copy().wait_send()
-        else:
-            pl.when(when)(lambda: copy().wait_send())
+    sent("sums", sum_out)
+    assert slots.used <= recv_sem.shape[0] and len(outgoing) <= send_sem.shape[0]
 
 
 def on_chip(sp_size, residual, queries, key_proj, value_proj, diff_lambda, head_gain, out_weight,
@@ -588,7 +600,7 @@
     hbm = pl.BlockSpec(memory_space=pltpu.HBM)
     vmem = pl.BlockSpec(memory_space=pltpu.VMEM)
     smem = pl.BlockSpec(memory_space=pltpu.SMEM)
-    copies = 256
+    receives, groups = 68, 12
     return pl.pallas_call(
         fused_kernel,
         out_shape=jax.ShapeDtypeStruct(residual.shape, BF16),
@@ -610,9 +622,9 @@
             pltpu.VMEM((3, units // 2, rows, span), BF16),
             pltpu.VMEM((4, units // 2, rows, span), BF16),
             pltpu.VMEM((rows, wide), F32),
-            pltpu.SemaphoreType.DMA((8,)),
-            pltpu.SemaphoreType.DMA((copies,)),
-            pltpu.SemaphoreType.DMA((copies,)),
+            pltpu.SemaphoreType.DMA((7,)),
+            pltpu.SemaphoreType.DMA((groups,)),
+            pltpu.SemaphoreType.DMA((receives,)),
         ],
         compiler_params=pltpu.CompilerParams(
             collective_id=0, has_side_effects=True, vmem_limit_bytes=60 * 2**20

time: 111 us -> 108 us (0.973)
  Pallas kernels: 110 us -> 106 us
    pallas_call x1, Pallas kernels: 110 us -> 106 us  [on_chip(): pl.pallas_call(fused_kernel, out_shape=jax.ShapeDtypeStruct(residual.shap...]
where the time goes in v4:
time: 108 us; the launch traced here: 107 us
  Pallas kernels  106 us (98%)
  local copies, waits for them, and re-layouts  1.67 us (2%)
    pallas_call x1, Pallas kernels, on_chip(): pl.pallas_call(fused_kernel, out_shape=jax.ShapeDtypeStruct(residual.shap...  106 us

profile of v4, /device:TPU:0, one launch (start us, length us, event | category | flops | bytes accessed | tf_op | source)
XLA Modules:
  0.0 107.4 jit_solution(10495056930134309857)
XLA Ops:
  0.0 105.8 %fused_layer.1 = bf16[128,1024]{1,0:T(8,128)(2,1)} custom-call(bf16[128,1024]{1,0:T(8,128)(2,1)} %residual.1, bf16[128,1024]{1,0:T(8,128)(2,1)} %queries.1, bf16[64,512]{1,0:T(8,128)(2,1)} %keys.1, bf16[64,512]{1,0:T(8,128)(2,1)} %values.1, f32[8]{0:T(128)} %lambdas.1, f32[1,256]{1,0:T(1,128)} %bitcast.3, bf16[2048,1024]{1,0:T(8,128)(2,1)} %out_weight.1, ...), custom_call_target="tpu_custom_call" | custom-call | tf_op jit(solution)/shard_map/fused_layer/pallas_call | solution.py:604
  105.8 1.7 %copy.12 = bf16[128,1024]{1,0:T(8,128)(2,1)} copy(bf16[128,1024]{1,0:T(8,128)(2,1)} %fused_layer.1) | data formatting | bytes 524288

commit v5 on v4

--- a/solution.py
+++ b/solution.py
@@ -134,7 +134,7 @@
     residual, queries, keys, values, lambdas, head_gain, out_weight, norm_gain,
     up, down, out,
     kv_all, up_all, down_all, q_buf, res_buf, w_buf, heads_all, squares, tokens, act,
-    parts, parts_in, sum_out, sum_in, after, local_sem, send_sem, recv_sem,
+    parts, parts_in, sum_out, sum_in, after, local_sem, send_sem, recv_sem, go,
 ):
     x = lax.axis_index("tp")
     s = lax.axis_index("sp")
@@ -422,7 +422,6 @@
     for k in (NEAR, FAR, MID):
         ups.pass_on(k)
     collect(0, is_outer)
-    deal(downs, down_chunk, FAR, is_outer)
     arrive(up_all.at[pl.ds(0, 2 * Z_CHIPS)], ups.twin)
 
     halves = up_all.shape[0] // 2
@@ -466,10 +465,23 @@
     activate(half)
     sent(("relay", 0), tokens.at[0], is_inner)
     sent(("relay", 1), squares.at[0], is_inner)
+
+    @pl.when(is_inner)
+    def _():
+        for peer in (across, beyond):
+            pl.semaphore_signal(go, inc=1, device_id=peer, device_id_type=MESH)
+        pl.semaphore_wait(go, 1)
+
     deal(downs, down_chunk, FAR, is_inner)
     downs.wait_twin(OWN, 0)
     project(OWN, 0, 0, keeps_far)
     downs.spread(1, is_inner | keeps_far)
+
+    @pl.when(is_outer)
+    def _():
+        pl.semaphore_wait(go, 1)
+
+    deal(downs, down_chunk, FAR, is_outer)
     collect(1, is_outer)
     downs.pass_on(OWN)
     downs.wait_twin(OWN, 1)
@@ -625,6 +637,7 @@
             pltpu.SemaphoreType.DMA((7,)),
             pltpu.SemaphoreType.DMA((groups,)),
             pltpu.SemaphoreType.DMA((receives,)),
+            pltpu.SemaphoreType.REGULAR,
         ],
         compiler_params=pltpu.CompilerParams(
             collective_id=0, has_side_effects=True, vmem_limit_bytes=60 * 2**20

time: 108 us -> 106 us (0.981)
  Pallas kernels: 106 us -> 104 us
    pallas_call x1, Pallas kernels: 106 us -> 104 us  [on_chip(): pl.pallas_call(fused_kernel, out_shape=jax.ShapeDtypeStruct(residual.shap...]
where the time goes in v5:
time: 106 us
  Pallas kernels  104 us (98%)
  local copies, waits for them, and re-layouts  1.67 us (2%)
    pallas_call x1, Pallas kernels, on_chip(): pl.pallas_call(fused_kernel, out_shape=jax.ShapeDtypeStruct(residual.shap...  104 us

profile of v5, /device:TPU:0, one launch (start us, length us, event | category | flops | bytes accessed | tf_op | source)
XLA Modules:
  0.0 105.8 jit_solution(5634361490238702538)
XLA Ops:
  0.0 104.2 %fused_layer.1 = bf16[128,1024]{1,0:T(8,128)(2,1)} custom-call(bf16[128,1024]{1,0:T(8,128)(2,1)} %residual.1, bf16[128,1024]{1,0:T(8,128)(2,1)} %queries.1, bf16[64,512]{1,0:T(8,128)(2,1)} %keys.1, bf16[64,512]{1,0:T(8,128)(2,1)} %values.1, f32[8]{0:T(128)} %lambdas.1, f32[1,256]{1,0:T(1,128)} %bitcast.3, bf16[2048,1024]{1,0:T(8,128)(2,1)} %out_weight.1, ...), custom_call_target="tpu_custom_call" | custom-call | tf_op jit(solution)/shard_map/fused_layer/pallas_call | solution.py:616
  104.2 1.7 %copy.12 = bf16[128,1024]{1,0:T(8,128)(2,1)} copy(bf16[128,1024]{1,0:T(8,128)(2,1)} %fused_layer.1) | data formatting | bytes 524288

commit v6 on v5

--- a/solution.py
+++ b/solution.py
@@ -408,8 +408,9 @@
     send_tokens(z, near, token_z)
     send_tokens(z, across, token_z + 4 - 2 * inner)
     send_tokens(z, mate, token_x)
-    deal(downs, down_chunk, NEAR, is_outer | keeps_far)
+    deal(downs, down_chunk, NEAR, keeps_far)
     deal(downs, down_chunk, MID)
+    deal(downs, down_chunk, NEAR, is_outer & sends_far)
     ups.spread(FAR, is_outer)
     ups.spread(MID, is_outer)
     down_own.wait()

time: 106 us -> 106 us (level)
  no operation moved by 1% of the time
where the time goes in v6:
time: 106 us
  Pallas kernels  104 us (98%)
  local copies, waits for them, and re-layouts  1.67 us (2%)
    pallas_call x1, Pallas kernels, on_chip(): pl.pallas_call(fused_kernel, out_shape=jax.ShapeDtypeStruct(residual.shap...  104 us

profile of v6, /device:TPU:0, one launch (start us, length us, event | category | flops | bytes accessed | tf_op | source)
XLA Modules:
  0.0 105.8 jit_solution(11810291615820557326)
XLA Ops:
  0.0 104.2 %fused_layer.1 = bf16[128,1024]{1,0:T(8,128)(2,1)} custom-call(bf16[128,1024]{1,0:T(8,128)(2,1)} %residual.1, bf16[128,1024]{1,0:T(8,128)(2,1)} %queries.1, bf16[64,512]{1,0:T(8,128)(2,1)} %keys.1, bf16[64,512]{1,0:T(8,128)(2,1)} %values.1, f32[8]{0:T(128)} %lambdas.1, f32[1,256]{1,0:T(1,128)} %bitcast.3, bf16[2048,1024]{1,0:T(8,128)(2,1)} %out_weight.1, ...), custom_call_target="tpu_custom_call" | custom-call | tf_op jit(solution)/shard_map/fused_layer/pallas_call | solution.py:617
  104.2 1.7 %copy.12 = bf16[128,1024]{1,0:T(8,128)(2,1)} copy(bf16[128,1024]{1,0:T(8,128)(2,1)} %fused_layer.1) | data formatting | bytes 524288
